TPU v7x, 32 devices: a whole 2x2x4 slice. The times are simulated.
32 devices in a mesh: ep: 8 (over z, x), tp: 4 (over y, core).
Axes of the slice: x: 2, y: 2, z: 4, core: 2. Of those that a mesh axis runs over, the one named last changes fastest.
Arguments:
- head_inputs_unfiltered: bfloat16 [1024, 4096], P('ep', 'tp'), may hold values from -6 to 6
- group_write_vectors: bfloat16 [1024, 512], P('ep', 'tp'), may hold values from -6 to 6
- group_read_vectors: bfloat16 [1024, 512], P('ep', 'tp'), may hold values from -6 to 6
- output_gate_inputs: bfloat16 [1024, 4096], P('ep', 'tp'), may hold values from -6 to 6
- step_preactivation: float32 [64, 1024], P('tp', 'ep'), may hold values from -3.2 to 3.6
- extra_decay_logs: float32 [64, 1024], P('tp', 'ep'), may hold values from -0.7 to 0
- head_decay_logs: float32 [64], P('tp'), may hold values from -16 to -2.7
- head_filter_taps: bfloat16 [4, 4096], P(None, 'tp'), may hold values from -3 to 3
- write_filter_taps: bfloat16 [4, 512], P(None, 'tp'), may hold values from -3 to 3
- read_filter_taps: bfloat16 [4, 512], P(None, 'tp'), may hold values from -3 to 3
- grouped_norm_gain: float32 [4096], P('tp'), may hold values from 0.1 to 1.9
- mixer_output_weight: bfloat16 [4096, 2048], P('tp'), may hold values from -0.09375 to 0.09375
- expert_input_rows: bfloat16 [4096, 2048], P(('ep', 'tp')), may hold values from -6 to 6
- expert_norm_gain: float32 [2048], replicated, may hold values from 0.1 to 1.9
- routes: int32 [4096, 2], P(('ep', 'tp')), may hold values from 0 to 7, all different within a row; in each aligned block of 128 rows (0 to 127, 128 to 255, ...) at most 48 rows name the same one
- router_chosen_scores: bfloat16 [4096, 2], P(('ep', 'tp')), may hold values from 0.049804688 to 1
- routed_gate_weight: bfloat16 [8, 2048, 1024], P('ep', None, 'tp'), may hold values from -0.125 to 0.125
- routed_up_weight: bfloat16 [8, 2048, 1024], P('ep', None, 'tp'), may hold values from -0.125 to 0.125
- routed_down_weight: bfloat16 [8, 1024, 2048], P('ep', 'tp'), may hold values from -0.1875 to 0.1875
- shared_gate_weight: bfloat16 [2048, 512], P(None, 'tp'), may hold values from -0.125 to 0.125
- shared_up_weight: bfloat16 [2048, 512], P(None, 'tp'), may hold values from -0.125 to 0.125
- shared_down_weight: bfloat16 [512, 2048], P('tp'), may hold values from -0.25 to 0.25
Outputs:
- mixer_result: bfloat16 [1024, 2048], P(('ep', 'tp'))
- moe_result: bfloat16 [4096, 2048], P(('ep', 'tp'))
Inputs may be any that keep to these rules, and one draw needn't show every extreme that they name: `routes`: within the 128 rows of one device no expert is named more than 48 times; a row names 2 different experts.
All inputs are finite; a program needn't handle non-finite values.
Results may differ from a plain program's by a relative error of at most 0.0095.
Values may be sent and summed in bfloat16 or wider, within the bound.
A program may use at most 128 MiB of HBM per device.

v0:
```python
import jax
import jax.numpy as jnp
from jax import lax
from jax.sharding import PartitionSpec as P

HEAD_DIM = 64
STATE = 128
BLOCK = 64


eps_norm = 1e-06
route_scale = 2.5
highest = lax.Precision.HIGHEST


def from_behind(value, axis, by):
    devices = lax.axis_size(axis)
    pairs = [(i, i + by) for i in range(devices) if 0 <= i + by < devices]
    return lax.ppermute(value, axis, pairs)


def carried_in(value, axis, join, neutral):
    count, mine = (lax.axis_size(axis), lax.axis_index(axis))
    pieces = jax.tree.map(lambda part: lax.all_gather(part, axis), value)
    running = jax.tree.map(
        lambda part, zero: jnp.full_like(part, 0) + jnp.asarray(zero, part.dtype), value, neutral
    )

    def step(position, running):
        longer = join(running, jax.tree.map(lambda part: part[position], pieces))
        return jax.tree.map(lambda new, old: jnp.where(position < mine, new, old), longer, running)

    return lax.fori_loop(0, count - 1, step, running)


def conv_silu(values, weights):
    taps = weights.shape[0]
    length = values.shape[0] - taps + 1
    running_sum = jnp.zeros((length, values.shape[1]), jnp.float32)
    for offset in range(taps):
        running_sum = running_sum + weights[offset].astype(jnp.float32) * values[
            offset : offset + length
        ].astype(jnp.float32)
    return jax.nn.silu(running_sum)


def combine_states(earlier_part, later_part):
    return (
        earlier_part[0] + later_part[0],
        later_part[1] + jnp.exp(later_part[0])[..., None, None] * earlier_part[1],
    )


def mixer_rows(
    head_inputs_unfiltered,
    group_write_vectors,
    group_read_vectors,
    output_gate_inputs,
    step_preactivation,
    extra_decay_logs,
    head_decay_logs,
    head_filter_taps,
    write_filter_taps,
    read_filter_taps,
    grouped_norm_gain,
):
    row_total = head_inputs_unfiltered.shape[0]
    taps = head_filter_taps.shape[0]
    head_chans = head_inputs_unfiltered.shape[1]
    write_chans = group_write_vectors.shape[1]
    tail_rows = jnp.concatenate(
        [
            head_inputs_unfiltered[row_total - taps + 1 :],
            group_write_vectors[row_total - taps + 1 :],
            group_read_vectors[row_total - taps + 1 :],
        ],
        axis=1,
    )
    earlier = from_behind(tail_rows, "ep", 1)
    padded_heads = jnp.concatenate([earlier[:, :head_chans], head_inputs_unfiltered], axis=0)
    padded_write = jnp.concatenate(
        [earlier[:, head_chans : head_chans + write_chans], group_write_vectors], axis=0
    )
    padded_read = jnp.concatenate(
        [earlier[:, head_chans + write_chans :], group_read_vectors], axis=0
    )
    heads_local = step_preactivation.shape[0]
    groups_local = write_chans // STATE
    per_group = heads_local // groups_local
    block_count = row_total // BLOCK
    head_values = conv_silu(padded_heads, head_filter_taps).reshape(
        block_count, BLOCK, groups_local, per_group, HEAD_DIM
    )
    write_values = conv_silu(padded_write, write_filter_taps).reshape(
        block_count, BLOCK, groups_local, STATE
    )
    read_values = conv_silu(padded_read, read_filter_taps).reshape(
        block_count, BLOCK, groups_local, STATE
    )
    step_length_value = jax.nn.softplus(step_preactivation)
    decay_rate_logs = -jnp.exp(head_decay_logs)[:, None] * step_length_value + extra_decay_logs
    step_blocks = step_length_value.reshape(groups_local, per_group, block_count, BLOCK)
    cumulative = jnp.cumsum(
        decay_rate_logs.reshape(groups_local, per_group, block_count, BLOCK), axis=3
    )
    weighted = head_values * jnp.transpose(step_blocks, (2, 3, 0, 1))[..., None]
    lower_mask = jnp.tril(jnp.ones((BLOCK, BLOCK), bool))
    gap_logs = cumulative[..., :, None] - cumulative[..., None, :]
    within = jnp.exp(jnp.where(lower_mask, gap_logs, -jnp.inf))
    affinity = jnp.einsum("blgn,bsgn->gbls", read_values, write_values, precision=highest)
    local_part = jnp.einsum(
        "gebls,bsgep->blgep", affinity[:, None] * within, weighted, precision=highest
    )
    to_end = jnp.exp(cumulative[..., -1:] - cumulative)
    block_states = jnp.einsum(
        "bsgn,bsgep,gebs->bgepn", write_values, weighted, to_end, precision=highest
    )
    block_decay = cumulative[..., -1]
    running = jnp.cumsum(block_decay, axis=2)
    entering = running - block_decay
    earlier_blocks = jnp.tril(jnp.ones((block_count, block_count), bool), -1)
    block_ratio = entering[..., :, None] - running[..., None, :]
    carry_weights = jnp.exp(jnp.where(earlier_blocks, block_ratio, -jnp.inf))
    inside = jnp.einsum("gebc,cgepn->bgepn", carry_weights, block_states, precision=highest)
    device_decay = running[..., -1]
    device_state = jnp.einsum(
        "gec,cgepn->gepn",
        jnp.exp(device_decay[..., None] - running),
        block_states,
        precision=highest,
    )
    scanned_pair = carried_in(
        (device_decay, device_state),
        "ep",
        combine_states,
        (jnp.zeros_like(device_decay), jnp.zeros_like(device_state)),
    )
    incoming = scanned_pair[1]
    states_in = (
        inside + jnp.exp(jnp.transpose(entering, (2, 0, 1)))[..., None, None] * incoming[None]
    )
    carried_part = (
        jnp.einsum("blgn,bgepn->blgep", read_values, states_in, precision=highest)
        * jnp.transpose(jnp.exp(cumulative), (2, 3, 0, 1))[..., None]
    )
    scan_out = (local_part + carried_part).reshape(row_total, groups_local, per_group * HEAD_DIM)
    gate_values = jax.nn.silu(output_gate_inputs.astype(jnp.float32)).reshape(
        row_total, groups_local, per_group * HEAD_DIM
    )
    gated_rows = scan_out * gate_values
    gated_rows = gated_rows * lax.rsqrt(
        jnp.mean(gated_rows * gated_rows, axis=-1, keepdims=True) + eps_norm
    )
    return (gated_rows.reshape(row_total, head_chans) * grouped_norm_gain).astype(jnp.bfloat16)


def local(
    head_inputs_unfiltered,
    group_write_vectors,
    group_read_vectors,
    output_gate_inputs,
    step_preactivation,
    extra_decay_logs,
    head_decay_logs,
    head_filter_taps,
    write_filter_taps,
    read_filter_taps,
    grouped_norm_gain,
    mixer_output_weight,
    expert_input_rows,
    expert_norm_gain,
    routes,
    router_chosen_scores,
    routed_gate_weight,
    routed_up_weight,
    routed_down_weight,
    shared_gate_weight,
    shared_up_weight,
    shared_down_weight,
):
    mixer_normed = mixer_rows(
        head_inputs_unfiltered,
        group_write_vectors,
        group_read_vectors,
        output_gate_inputs,
        step_preactivation,
        extra_decay_logs,
        head_decay_logs,
        head_filter_taps,
        write_filter_taps,
        read_filter_taps,
        grouped_norm_gain,
    )
    tp_count = lax.axis_size("tp")
    tp_index = lax.axis_index("tp")
    ep_count = lax.axis_size("ep")
    tok_local = expert_input_rows.shape[0]
    model_width = expert_input_rows.shape[1]
    top_count = routes.shape[1]
    local_experts = routed_gate_weight.shape[0]
    experts = local_experts * ep_count
    capacity = 3 * tok_local * top_count // (2 * experts)
    rows_float = expert_input_rows.astype(jnp.float32)
    normed = (
        rows_float
        * lax.rsqrt(jnp.mean(rows_float * rows_float, axis=-1, keepdims=True) + eps_norm)
        * expert_norm_gain
    ).astype(jnp.bfloat16)
    group_rows, group_routes, group_scores = (
        lax.all_gather(normed, "tp", axis=0, tiled=True),
        lax.all_gather(routes, "tp", axis=0, tiled=True),
        lax.all_gather(router_chosen_scores, "tp", axis=0, tiled=True),
    )
    score_float = group_scores.astype(jnp.float32)
    weights = score_float / jnp.sum(score_float, axis=1, keepdims=True) * route_scale
    group_count = group_rows.shape[0]
    by_owner = group_routes.reshape(tp_count, tok_local * top_count)
    onehot = (by_owner[:, :, None] == jnp.arange(experts, dtype=jnp.int32)[None, None, :]).astype(
        jnp.int32
    )
    before = jnp.cumsum(onehot, axis=1) - onehot
    slot_rank = jnp.sum(before * onehot, axis=2)
    owner_base = jnp.arange(tp_count, dtype=jnp.int32)[:, None] * (experts * capacity)
    slot_index = owner_base + by_owner * capacity + slot_rank
    flat_slot = slot_index.reshape(-1)
    own_slot = lax.dynamic_index_in_dim(slot_index, tp_index, 0, keepdims=False) - tp_index * (
        experts * capacity
    )
    shared_hidden = (
        jax.nn.silu(jnp.dot(group_rows, shared_gate_weight, preferred_element_type=jnp.float32))
        * jnp.dot(group_rows, shared_up_weight, preferred_element_type=jnp.float32)
    ).astype(jnp.bfloat16)
    shared_part = jnp.dot(shared_hidden, shared_down_weight, preferred_element_type=jnp.float32)
    token_of = jnp.arange(group_count * top_count, dtype=jnp.int32) // top_count
    slot_token = (
        jnp.full((tp_count * experts * capacity,), group_count, jnp.int32)
        .at[flat_slot]
        .set(token_of)
    )
    padded_rows = jnp.concatenate([group_rows, jnp.zeros((1, model_width), jnp.bfloat16)], axis=0)
    outgoing = padded_rows[slot_token].reshape(tp_count, experts, capacity, model_width)
    arrived = lax.all_to_all(outgoing, "ep", split_axis=1, concat_axis=1, tiled=True)
    sources = arrived.reshape(tp_count, ep_count, local_experts, capacity, model_width)
    gate_value = jnp.einsum(
        "osecd,edf->osecf", sources, routed_gate_weight, preferred_element_type=jnp.float32
    )
    up_value = jnp.einsum(
        "osecd,edf->osecf", sources, routed_up_weight, preferred_element_type=jnp.float32
    )
    hidden = (jax.nn.silu(gate_value) * up_value).astype(jnp.bfloat16)
    partial_value = jnp.einsum(
        "osecf,efd->osecd", hidden, routed_down_weight, preferred_element_type=jnp.float32
    ).astype(jnp.bfloat16)
    slot_rows = ep_count * local_experts * capacity
    flat_partial = partial_value.reshape(tp_count * slot_rows, model_width)
    summed = lax.psum_scatter(
        flat_partial.astype(jnp.float32).astype(jnp.bfloat16), "tp", scatter_dimension=0, tiled=True
    ).astype(jnp.float32)
    returned_sums = lax.all_to_all(
        summed.reshape(ep_count * local_experts, capacity, model_width),
        "ep",
        split_axis=0,
        concat_axis=0,
        tiled=True,
    )
    own_weights = lax.dynamic_slice_in_dim(weights, tp_index * tok_local, tok_local, 0)
    picked = returned_sums.reshape(-1, model_width)[own_slot].reshape(
        tok_local, top_count, model_width
    )
    own_term = jnp.sum(picked * own_weights[:, :, None], axis=1)
    mix_block = mixer_normed.shape[0] // tp_count
    block_rows = mix_block + tok_local
    part_count = lax.axis_size("tp") * block_rows // block_rows
    mix_term = jnp.dot(
        mixer_normed, mixer_output_weight, preferred_element_type=jnp.float32
    ).reshape(part_count, mix_block, model_width)
    moe_term = shared_part.reshape(part_count, tok_local, model_width)
    row_sums = lax.psum_scatter(
        jnp.concatenate([mix_term, moe_term], axis=1).reshape(
            lax.axis_size("tp") * block_rows, model_width
        ),
        "tp",
        scatter_dimension=0,
        tiled=True,
    )
    mixer_result = row_sums[:mix_block].astype(jnp.bfloat16)
    moe_sum = row_sums[mix_block:]
    moe_total = moe_sum + own_term
    return (mixer_result, moe_total.astype(jnp.bfloat16))


def solution(mesh):
    in_specs = (
        P("ep", "tp"),
        P("ep", "tp"),
        P("ep", "tp"),
        P("ep", "tp"),
        P("tp", "ep"),
        P("tp", "ep"),
        P("tp"),
        P(None, "tp"),
        P(None, "tp"),
        P(None, "tp"),
        P("tp"),
        P("tp", None),
        P(("ep", "tp"), None),
        P(),
        P(("ep", "tp"), None),
        P(("ep", "tp"), None),
        P("ep", None, "tp"),
        P("ep", None, "tp"),
        P("ep", "tp", None),
        P(None, "tp"),
        P(None, "tp"),
        P("tp", None),
    )
    out_specs = (P(("ep", "tp"), None), P(("ep", "tp"), None))
    return jax.shard_map(local, mesh=mesh, in_specs=in_specs, out_specs=out_specs, check_vma=False)
```

profile of v0, /device:TPU:0, one launch (start us, length us, event | category | flops | bytes accessed | tf_op | source)
XLA Modules:
  0.0 392.0 jit_solution(7887876798861963684)
XLA Ops:
  8.1 1.3 fusion.24
  9.4 2.0 fusion.26
  11.4 6.3 %all_gather.22 = s32[512,2]{0,1:T(2,128)S(1)} all-gather(s32[128,2]{0,1:T(2,128)} %param.38), channel_id=1, replica_groups=mesh['ep'=8,'tp'=4] {'tp'}, dimensions={0}, use_global_device_ids=true | all-gather | bytes 5120 | tf_op jit(solution)/shard_map/all_gather | solution.py:211
  18.3 2.3 reduce-window.6
  21.3 4.3 %scatter_custom_fusion = s32[1536]{0:T(1024)S(1)} fusion(s32[1024]{0:T(1024)S(1)} %bitcast.253, s32[1024]{0:T(1024)S(1)} %add_select_fusion, s32[]{:T(128)} %constant.110.clone.1), kind=kCustom, calls=%fused_computation.134 | custom fusion | bytes 6148 | tf_op jit(solution)/shard_map/scatter | solution.py:238
  25.7 11.3 %all-gather.5.cloned.1.call-done = bf16[512,2048]{1,0:T(8,128)(2,1)} async-done(((bf16[128,2048]{1,0:T(8,128)(2,1)}), bf16[512,2048]{1,0:T(8,128)(2,1)}) %all-gather.5.cloned.1.call-update) | async-done | bytes 2097168 | tf_op jit(solution)/shard_map/all_gather | solution.py:210
  36.9 1.7 concatenate.23
  38.7 7.1 %gather_fusion = bf16[1536,2048]{1,0:T(8,128)(2,1)} fusion(bf16[513,2048]{1,0:T(8,128)(2,1)S(1)} %concatenate.23, s32[2048]{0:T(1024)S(1)} %pad_clamp_fusion), kind=kCustom, calls=%fused_computation | custom fusion | bytes 12589056 | tf_op jit(solution)/shard_map/gather | solution.py:241
  45.8 6.6 %copy.71 = bf16[4,8,48,2048]{3,2,0,1:T(8,128)(2,1)} copy(bf16[4,8,48,2048]{3,2,1,0:T(8,128)(2,1)} %bitcast.225) | data formatting | bytes 12582912 | tf_op jit(solution)/shard_map/reshape | solution.py:241
  52.4 5.6 %all-to-all-start = ((bf16[4,8,48,2048]{3,2,0,1:T(8,128)(2,1)}), bf16[4,8,48,2048]{3,2,0,1:T(8,128)(2,1)}, u32[]{:S(2)}, u32[]{:S(2)}) async-start(bf16[4,8,48,2048]{3,2,0,1:T(8,128)(2,1)} %copy.71), calls=%async_computation.1 | async-start | bytes 12582912 | tf_op jit(solution)/shard_map/all_to_all | solution.py:242
  58.2 3.9 collective-permute-start
  63.3 46.1 %collective-permute-done = bf16[3,1280]{1,0:T(4,128)(2,1)S(1)} collective-permute-done((bf16[3,1280]{1,0:T(4,128)(2,1)S(1)}, bf16[3,1280]{1,0:T(4,128)(2,1)S(1)}, u32[]{:S(2)}, u32[]{:S(2)}) %collective-permute-start) | collective-permute-done | bytes 7712 | tf_op jit(solution)/shard_map/ppermute | solution.py:19
  110.6 1.1 fusion.32
  111.7 1.0 copy-done.7
  112.7 4.5 %fusion.40 = f32[16,1,64,128]{3,1,2,0:T(1,128)} fusion(f32[16,2,1,1]{1,2,3,0:T(1,128)S(1)} %copy.77, f32[2,16,64,128]{3,2,1,0:T(8,128)S(1)} %fusion.32), kind=kOutput, calls=%fused_computation.52 | convolution fusion | flops 3145728 | bytes 1572992 | tf_op jit(solution)/shard_map/gec,cgepn->gepn/dot_general | solution.py:126
  117.5 79.2 %all-to-all-done = bf16[4,8,48,2048]{3,2,0,1:T(8,128)(2,1)} async-done(((bf16[4,8,48,2048]{3,2,0,1:T(8,128)(2,1)}), bf16[4,8,48,2048]{3,2,0,1:T(8,128)(2,1)}, u32[]{:S(2)}, u32[]{:S(2)}) %all-to-all-start) | async-done | bytes 6291488 | tf_op jit(solution)/shard_map/all_to_all | solution.py:242
  196.7 6.0 %fusion.3 = f32[4,8,48,256]{3,2,1,0:T(8,128)} fusion(bf16[4,8,48,2048]{3,2,0,1:T(8,128)(2,1)} %all-to-all-done, bf16[1,2048,256]{2,1,0:T(8,128)(2,1)} %param.40), kind=kOutput, calls=%fused_computation.8 | convolution fusion | flops 1610612736 | bytes 8912896 | tf_op jit(solution)/shard_map/osecd,edf->osecf/dot_general | solution.py:244
  202.7 12.6 %convolution_convert_fusion = bf16[4,8,48,2048]{3,2,1,0:T(8,128)(2,1)} fusion(bf16[4,8,48,2048]{3,2,0,1:T(8,128)(2,1)} %all-to-all-done, f32[4,8,48,256]{3,2,1,0:T(8,128)} %fusion.3, bf16[1,256,2048]{2,1,0:T(8,128)(2,1)S(1)} %copy-done, bf16[1,2048,256]{2,1,0:T(8,128)(2,1)} %param.41), kind=kOutput, calls=%fused_computation.11 | convolution fusion | flops 3226730496 | bytes 16252928 | tf_op jit(solution)/shard_map/osecf,efd->osecd/dot_general | solution.py:251
  215.9 22.3 %all-gather.1 = f32[8,16,1]{1,2,0:T(1,128)S(1)} all-gather(f32[1,16,1]{1,2,0:T(1,128)S(1)} %get-tuple-element.148), channel_id=3, replica_groups=mesh['ep'=8,'tp'=4] {'ep'}, dimensions={0}, use_global_device_ids=true | all-gather | bytes 576 | tf_op jit(solution)/shard_map/all_gather | solution.py:24
  238.6 1.7 fusion.97
  240.3 5.5 %fusion.23 = f32[512,2048]{1,0:T(8,128)} fusion(bf16[128,2048]{1,0:T(8,128)(2,1)} %param.45, bf16[512,2048]{1,0:T(8,128)(2,1)S(1)} %copy-done.2, bf16[2048,128]{1,0:T(8,128)(2,1)} %param.44, f32[512,128]{1,0:T(8,128)S(1)} %fusion.97), kind=kOutput, calls=%fused_computation.34 | convolution fusion | flops 537264128 | bytes 7602176 | tf_op jit(solution)/shard_map/dot_general | solution.py:233
  245.9 28.7 %all-gather.7.cloned.1.call-done = f32[128,64,128]{2,1,0:T(8,128)} async-done(((f32[16,64,128]{2,1,0:T(8,128)}), f32[128,64,128]{2,1,0:T(8,128)}) %all-gather.7.cloned.1.call-update) | async-done | bytes 4194320 | tf_op jit(solution)/shard_map/all_gather | solution.py:24
  274.5 8.6 %while.14 = (s32[]{:T(128)}, f32[1,16,64,128]{3,2,1,0:T(8,128)S(1)}, s32[]{:T(128)}, f32[8,1,16,64,128]{4,3,2,1,0:T(8,128)}, f32[8,1,16]{2,1,0:T(1,128)S(1)}, /*index=5*/s32[]{:T(128)}, s32[]{:T(128)}) while((s32[]{:T(128)}, f32[1,16,64,128]{3,2,1,0:T(8,128)S(1)}, s32[]{:T(128)}, f32[8,1,16,64,128]{4,3,2,1,0:T(8,128)}, ...), condition=%wide.region_3.4_spmd.clone, body=%wide.region_2.3_spmd.clone.sunk | while | flops 524292 | bytes 1573161 | solution.py:33
  274.5 1.3 fusion.109
  275.8 1.2 fusion.109
  277.1 1.2 fusion.109
  278.3 1.2 fusion.109
  279.5 1.2 fusion.109
  280.7 1.2 fusion.109
  281.9 1.2 fusion.109
  283.1 4.2 %fusion.21 = f32[2,16,64,128]{3,0,2,1:T(2,128)S(1)} fusion(f32[2,16,64,128]{3,2,1,0:T(8,128)S(1)} %copy-done.8, f32[16,64,128]{2,1,0:T(8,128)S(1)} %bitcast.228, f32[2,16]{0,1:T(8,128)S(1)} %copy.61, pred[2,2]{1,0:T(4,128)(4,1)S(1)} %iota_compare_fusion.3, f32[16,2]{1,0:T(8,128)S(1)} %copy.59, f32[16,2]{1,0:T(8,128)S(1)} %bitcast.250), kind=kOutput, calls=%fused_computation.31 | convolution fusion | flops 6815872 | bytes 2621828 | tf_op jit(solution)/shard_map/gebc,cgepn->bgepn/dot_general | solution.py:124
  287.4 1.0 fusion.14
  288.4 2.0 fusion.13
  290.5 0.5 copy.65
  291.8 3.1 fusion.5
  295.2 2.7 pad_maximum_fusion
  298.0 3.4 convert.25
  301.4 3.8 all-to-all-start.1
  305.2 0.6 dynamic-slice
  305.8 5.3 %all_gather.23 = bf16[512,2]{0,1:T(2,128)(2,1)S(1)} all-gather(bf16[128,2]{0,1:T(2,128)(2,1)S(1)} %copy-done.19), channel_id=1, replica_groups=mesh['ep'=8,'tp'=4] {'tp'}, dimensions={0}, use_global_device_ids=true | all-gather | bytes 2560 | tf_op jit(solution)/shard_map/all_gather | solution.py:212
  311.3 0.7 compare_select_fusion.3
  312.0 36.0 %reduce-scatter.3.cloned.1.call-done = f32[160,2048]{1,0:T(8,128)} async-done(((f32[640,2048]{1,0:T(8,128)}), f32[160,2048]{1,0:T(8,128)}) %reduce-scatter.3.cloned.1.call-update) | async-done | bytes 1310736 | tf_op jit(solution)/shard_map/reduce_scatter | solution.py:278
  348.1 1.6 slice.213
  349.7 25.8 %all-to-all-done.1 = f32[8,48,2048]{2,1,0:T(8,128)S(1)} async-done(((f32[8,48,2048]{2,1,0:T(8,128)}), f32[8,48,2048]{2,1,0:T(8,128)S(1)}, u32[]{:S(2)}, u32[]{:S(2)}) %all-to-all-start.1) | async-done | bytes 3145760 | tf_op jit(solution)/shard_map/all_to_all | solution.py:259
  375.5 2.7 gather_fusion.1
  378.2 2.6 reshape.347
  380.8 3.2 multiply_reduce_fusion
  384.0 0.9 fusion.27
  (127 shorter events, 6.3 us)
Async XLA Ops:
  8.0 194.7 %copy-start = (bf16[1,256,2048]{2,1,0:T(8,128)(2,1)S(1)}, bf16[1,256,2048]{2,1,0:T(8,128)(2,1)}, u32[]{:S(2)}) copy-start(bf16[1,256,2048]{2,1,0:T(8,128)(2,1)} %param.42) | copy-start | bytes 3145732
  8.0 28.9 %all-gather.5.cloned.1.call-start = ((), (), s32[]{:S(2)}) async-start(), calls=%async_computation.4 | async-start | bytes 2621440 | tf_op jit(solution)/shard_map/all_gather | solution.py:210
  52.4 5.7 %copy-start.10 = (bf16[128,1024]{1,0:T(8,128)(2,1)S(1)}, bf16[128,1024]{1,0:T(8,128)(2,1)}, u32[]{:S(2)}) copy-start(bf16[128,1024]{1,0:T(8,128)(2,1)} %param.24) | copy-start | bytes 786436
  52.4 5.8 %copy-start.12 = (bf16[128,128]{1,0:T(8,128)(2,1)S(1)}, bf16[128,128]{1,0:T(8,128)(2,1)}, u32[]{:S(2)}) copy-start(bf16[128,128]{1,0:T(8,128)(2,1)} %param.25) | copy-start | bytes 98308
  52.4 5.8 %copy-start.13 = (bf16[128,128]{1,0:T(8,128)(2,1)S(1)}, bf16[128,128]{1,0:T(8,128)(2,1)}, u32[]{:S(2)}) copy-start(bf16[128,128]{1,0:T(8,128)(2,1)} %param.26) | copy-start | bytes 98308
  52.4 9.7 %copy-start.20 = (f32[16]{0:T(128)S(1)}, f32[16]{0:T(128)}, u32[]{:S(2)}) copy-start(f32[16]{0:T(128)} %param.30) | copy-start | bytes 196
  52.4 9.7 %copy-start.15 = (f32[16,128]{1,0:T(8,128)S(1)}, f32[16,128]{1,0:T(8,128)}, u32[]{:S(2)}) copy-start(f32[16,128]{1,0:T(8,128)} %param.28) | copy-start | bytes 24580
  52.4 9.7 %copy-start.16 = (f32[16,128]{1,0:T(8,128)S(1)}, f32[16,128]{1,0:T(8,128)}, u32[]{:S(2)}) copy-start(f32[16,128]{1,0:T(8,128)} %param.29) | copy-start | bytes 24580
  52.4 10.5 %copy-start.17 = (bf16[4,128]{1,0:T(4,128)(2,1)S(1)}, bf16[4,128]{1,0:T(4,128)(2,1)}, u32[]{:S(2)}) copy-start(bf16[4,128]{1,0:T(4,128)(2,1)} %param.32) | copy-start | bytes 3076
  52.4 10.5 %copy-start.18 = (bf16[4,128]{1,0:T(4,128)(2,1)S(1)}, bf16[4,128]{1,0:T(4,128)(2,1)}, u32[]{:S(2)}) copy-start(bf16[4,128]{1,0:T(4,128)(2,1)} %param.33) | copy-start | bytes 3076
  52.4 10.5 %copy-start.14 = (bf16[4,1024]{1,0:T(4,128)(2,1)S(1)}, bf16[4,1024]{1,0:T(4,128)(2,1)}, u32[]{:S(2)}) copy-start(bf16[4,1024]{1,0:T(4,128)(2,1)} %param.31) | copy-start | bytes 24580
  52.4 144.2 %all-to-all-start = ((bf16[4,8,48,2048]{3,2,0,1:T(8,128)(2,1)}), bf16[4,8,48,2048]{3,2,0,1:T(8,128)(2,1)}, u32[]{:S(2)}, u32[]{:S(2)}) async-start(bf16[4,8,48,2048]{3,2,0,1:T(8,128)(2,1)} %copy.71), calls=%async_computation.1 | async-start | bytes 12582912 | tf_op jit(solution)/shard_map/all_to_all | solution.py:242
  58.0 216.5 %all-gather.7.cloned.1.call-start = ((), (), s32[]{:S(2)}) async-start(), calls=%async_computation.7 | async-start | bytes 4718592 | tf_op jit(solution)/shard_map/all_gather | solution.py:24
  58.2 51.2 %collective-permute-start = (bf16[3,1280]{1,0:T(4,128)(2,1)S(1)}, bf16[3,1280]{1,0:T(4,128)(2,1)S(1)}, u32[]{:S(2)}, u32[]{:S(2)}) collective-permute-start(bf16[3,1280]{1,0:T(4,128)(2,1)S(1)} %pad_maximum_fusion.4), channel_id=1, source_target_pairs={{0,4},{4,8},{8,12},{12,16},{16,20},{20,24},{24,28},{1,5},{5,9},{9,... | collective-permute-start | bytes 23048 | tf_op jit(solution)/shard_map/ppermute | solution.py:19
  110.5 92.2 %copy-start.4 = (f32[2,64,16,64]{1,3,2,0:T(8,128)}, f32[2,64,16,64]{1,3,2,0:T(8,128)S(1)}, u32[]{:S(2)}) copy-start(f32[2,64,16,64]{1,3,2,0:T(8,128)S(1)} %copy.55) | copy-start | bytes 1572868
  111.7 1.0 copy-start.7
  117.2 180.8 %reduce-scatter.5.cloned.1.call-start = ((), (), s32[]{:S(2)}) async-start(), calls=%async_computation.6 | async-start | bytes 7864320 | tf_op jit(solution)/shard_map/reduce_scatter | solution.py:256
  215.3 23.3 %copy-start.2 = (bf16[512,2048]{1,0:T(8,128)(2,1)S(1)}, bf16[512,2048]{1,0:T(8,128)(2,1)}, u32[]{:S(2)}) copy-start(bf16[512,2048]{1,0:T(8,128)(2,1)} %all-gather.5.cloned.1.call-done) | copy-start | bytes 6291460
  215.3 132.7 %reduce-scatter.3.cloned.1.call-start = ((), (), s32[]{:S(2)}) async-start(), calls=%async_computation.5 | async-start | bytes 6553600 | tf_op jit(solution)/shard_map/reduce_scatter | solution.py:278
  274.5 8.6 %copy-start.8 = (f32[2,16,64,128]{3,2,1,0:T(8,128)S(1)}, f32[2,16,64,128]{3,2,1,0:T(8,128)}, u32[]{:S(2)}) copy-start(f32[2,16,64,128]{3,2,1,0:T(8,128)} %copy-done.7) | copy-start | bytes 3145732
  283.1 5.3 %copy-start.5 = (f32[2,64,16,64]{1,3,2,0:T(8,128)S(1)}, f32[2,64,16,64]{1,3,2,0:T(8,128)}, u32[]{:S(2)}) copy-start(f32[2,64,16,64]{1,3,2,0:T(8,128)} %copy-done.4) | copy-start | bytes 1572868
  288.4 2.9 copy-start.9
  290.5 1.3 copy-start.11
  291.8 3.5 copy-start.3
  301.4 4.4 %copy-start.19 = (bf16[128,2]{0,1:T(2,128)(2,1)S(1)}, bf16[128,2]{0,1:T(2,128)(2,1)}, u32[]{:S(2)}) copy-start(bf16[128,2]{0,1:T(2,128)(2,1)} %param.39) | copy-start | bytes 1540
  301.4 74.1 %all-to-all-start.1 = ((f32[8,48,2048]{2,1,0:T(8,128)}), f32[8,48,2048]{2,1,0:T(8,128)S(1)}, u32[]{:S(2)}, u32[]{:S(2)}) async-start(f32[8,48,2048]{2,1,0:T(8,128)} %convert.25), calls=%async_computation.3 | async-start | bytes 6291456 | tf_op jit(solution)/shard_map/all_to_all | solution.py:259
  378.2 6.7 %copy-start.1 = (bf16[1,256,2048]{2,1,0:T(8,128)(2,1)S(1)}, bf16[1,256,2048]{2,1,0:T(8,128)(2,1)}, u32[]{:S(2)}) copy-start(bf16[1,256,2048]{2,1,0:T(8,128)(2,1)} %param.42) | copy-start | bytes 3145732
  380.8 3.2 copy-start.6
Sparse Core Ops, SparseCore 0:
  11.6 25.3 all-gather.4
  215.4 64.7 reduce-scatter.4
  298.1 49.9 reduce-scatter.2
Sparse Core Ops, SparseCore 1:
  117.3 157.2 all-gather.6
where the time goes:
time: 393 us; the launch traced here: 392 us
  waiting for transfers between devices  227 us (58%)
  matrix products  42 us (11%)
  blocking collectives  33.9 us (9%)
  local copies, waits for them, and re-layouts  32.5 us (8%)
  other arithmetic  26.8 us (7%)
  between operations  15.8 us (4%)
  starting transfers between devices  13.6 us (3%)
    all_to_all x1, waiting for transfers between devices, local(): lax.all_to_all(outgoing, 'ep', split_axis=1, concat_axis=1, tiled=True)  79.2 us
    ppermute x1, waiting for transfers between devices, from_behind(): return lax.ppermute(value, axis, pairs)  46.1 us
    reduce_scatter x1, waiting for transfers between devices, local(): lax.psum_scatter(jnp.concatenate([mix_term, moe_term], axis=1).reshape(la...  36 us
    all_gather x1, waiting for transfers between devices, carried_in(): pieces = jax.tree.map(lambda part: lax.all_gather(part, axis), value)  28.7 us
    all_to_all x1, waiting for transfers between devices, local(): lax.all_to_all(summed.reshape(ep_count * local_experts, capacity, model_w...  25.8 us
    all_gather x1, blocking collectives, carried_in(): pieces = jax.tree.map(lambda part: lax.all_gather(part, axis), value)  22.3 us
    dot_general x1, matrix products, local(): jnp.einsum('osecf,efd->osecd', hidden, routed_down_weight, preferred_elem...  12.6 us
    all_gather x1, waiting for transfers between devices, local(): lax.all_gather(normed, 'tp', axis=0, tiled=True)  11.3 us
  transfers between devices with their start and end apart: 7, of which 6 were waited for; matrix products, arithmetic and copies ran while one was open for 18% of the time, Pallas kernels for 0%

commit v1 on v0

v1 whole, which is shorter than its diff:
```python
import jax
import jax.numpy as jnp
from jax import lax
from jax.sharding import PartitionSpec as P

HEAD_DIM = 64
STATE = 128
BLOCK = 64


eps_norm = 1e-06
route_scale = 2.5
highest = lax.Precision.HIGHEST


def from_behind(value, axis, by):
    devices = lax.axis_size(axis)
    pairs = [(i, i + by) for i in range(devices) if 0 <= i + by < devices]
    return lax.ppermute(value, axis, pairs)


def carried_in(decay, state, axis):
    count, mine = (lax.axis_size(axis), lax.axis_index(axis))
    heads = decay.size
    width = state.shape[-1]
    flat_decay = decay.reshape(heads)
    parts, rest = [], flat_decay
    for _ in range(3):
        part = lax.reduce_precision(rest, exponent_bits=8, mantissa_bits=7)
        parts.append(part)
        rest = rest - part
    decay_rows = jnp.pad(jnp.stack(parts, axis=1), ((0, 0), (0, width - 3)))
    packed = jnp.concatenate([state.reshape(-1, width), decay_rows], axis=0).astype(jnp.bfloat16)
    pieces = lax.all_gather(packed, axis).astype(jnp.float32)
    decays = jnp.sum(pieces[:, -heads:, :3], axis=-1)
    order = jnp.arange(count, dtype=jnp.int32)
    between = (order[None, :] > order[:, None]) & (order[None, :] < mine)
    spans = jnp.sum(jnp.where(between[:, :, None], decays[None], 0.0), axis=1)
    ratio = jnp.where((order < mine)[:, None], jnp.exp(spans), 0.0)
    states = pieces[:, :-heads].reshape((count, heads) + state.shape[-2:])
    return jnp.sum(states * ratio[:, :, None, None], axis=0).reshape(state.shape)


def conv_silu(values, weights):
    taps = weights.shape[0]
    length = values.shape[0] - taps + 1
    running_sum = jnp.zeros((length, values.shape[1]), jnp.float32)
    for offset in range(taps):
        running_sum = running_sum + weights[offset].astype(jnp.float32) * values[
            offset : offset + length
        ].astype(jnp.float32)
    return jax.nn.silu(running_sum)


def tail_rows_from_behind(head_inputs, write_vectors, read_vectors, taps):
    start = head_inputs.shape[0] - taps + 1
    tail_rows = jnp.concatenate([head_inputs[start:], write_vectors[start:], read_vectors[start:]], axis=1)
    return from_behind(tail_rows, "ep", 1)


def mixer_rows(
    earlier,
    head_inputs_unfiltered,
    group_write_vectors,
    group_read_vectors,
    output_gate_inputs,
    step_preactivation,
    extra_decay_logs,
    head_decay_logs,
    head_filter_taps,
    write_filter_taps,
    read_filter_taps,
    grouped_norm_gain,
):
    row_total = head_inputs_unfiltered.shape[0]
    head_chans = head_inputs_unfiltered.shape[1]
    write_chans = group_write_vectors.shape[1]
    padded_heads = jnp.concatenate([earlier[:, :head_chans], head_inputs_unfiltered], axis=0)
    padded_write = jnp.concatenate(
        [earlier[:, head_chans : head_chans + write_chans], group_write_vectors], axis=0
    )
    padded_read = jnp.concatenate(
        [earlier[:, head_chans + write_chans :], group_read_vectors], axis=0
    )
    heads_local = step_preactivation.shape[0]
    groups_local = write_chans // STATE
    per_group = heads_local // groups_local
    block_count = row_total // BLOCK
    head_values = conv_silu(padded_heads, head_filter_taps).reshape(
        block_count, BLOCK, groups_local, per_group, HEAD_DIM
    )
    write_values = conv_silu(padded_write, write_filter_taps).reshape(
        block_count, BLOCK, groups_local, STATE
    )
    read_values = conv_silu(padded_read, read_filter_taps).reshape(
        block_count, BLOCK, groups_local, STATE
    )
    step_length_value = jax.nn.softplus(step_preactivation)
    decay_rate_logs = -jnp.exp(head_decay_logs)[:, None] * step_length_value + extra_decay_logs
    step_blocks = step_length_value.reshape(groups_local, per_group, block_count, BLOCK)
    cumulative = jnp.cumsum(
        decay_rate_logs.reshape(groups_local, per_group, block_count, BLOCK), axis=3
    )
    weighted = head_values * jnp.transpose(step_blocks, (2, 3, 0, 1))[..., None]
    lower_mask = jnp.tril(jnp.ones((BLOCK, BLOCK), bool))
    gap_logs = cumulative[..., :, None] - cumulative[..., None, :]
    within = jnp.exp(jnp.where(lower_mask, gap_logs, -jnp.inf))
    affinity = jnp.einsum("blgn,bsgn->gbls", read_values, write_values, precision=highest)
    local_part = jnp.einsum(
        "gebls,bsgep->blgep", affinity[:, None] * within, weighted, precision=highest
    )
    to_end = jnp.exp(cumulative[..., -1:] - cumulative)
    block_states = jnp.einsum(
        "bsgn,bsgep,gebs->bgepn", write_values, weighted, to_end, precision=highest
    )
    block_decay = cumulative[..., -1]
    running = jnp.cumsum(block_decay, axis=2)
    entering = running - block_decay
    earlier_blocks = jnp.tril(jnp.ones((block_count, block_count), bool), -1)
    block_ratio = entering[..., :, None] - running[..., None, :]
    carry_weights = jnp.exp(jnp.where(earlier_blocks, block_ratio, -jnp.inf))
    inside = jnp.einsum("gebc,cgepn->bgepn", carry_weights, block_states, precision=highest)
    device_decay = running[..., -1]
    device_state = jnp.einsum(
        "gec,cgepn->gepn",
        jnp.exp(device_decay[..., None] - running),
        block_states,
        precision=highest,
    )
    incoming = carried_in(device_decay, device_state, "ep")
    states_in = (
        inside + jnp.exp(jnp.transpose(entering, (2, 0, 1)))[..., None, None] * incoming[None]
    )
    carried_part = (
        jnp.einsum("blgn,bgepn->blgep", read_values, states_in, precision=highest)
        * jnp.transpose(jnp.exp(cumulative), (2, 3, 0, 1))[..., None]
    )
    scan_out = (local_part + carried_part).reshape(row_total, groups_local, per_group * HEAD_DIM)
    gate_values = jax.nn.silu(output_gate_inputs.astype(jnp.float32)).reshape(
        row_total, groups_local, per_group * HEAD_DIM
    )
    gated_rows = scan_out * gate_values
    gated_rows = gated_rows * lax.rsqrt(
        jnp.mean(gated_rows * gated_rows, axis=-1, keepdims=True) + eps_norm
    )
    return (gated_rows.reshape(row_total, head_chans) * grouped_norm_gain).astype(jnp.bfloat16)


def local(
    head_inputs_unfiltered,
    group_write_vectors,
    group_read_vectors,
    output_gate_inputs,
    step_preactivation,
    extra_decay_logs,
    head_decay_logs,
    head_filter_taps,
    write_filter_taps,
    read_filter_taps,
    grouped_norm_gain,
    mixer_output_weight,
    expert_input_rows,
    expert_norm_gain,
    routes,
    router_chosen_scores,
    routed_gate_weight,
    routed_up_weight,
    routed_down_weight,
    shared_gate_weight,
    shared_up_weight,
    shared_down_weight,
):
    earlier = tail_rows_from_behind(
        head_inputs_unfiltered, group_write_vectors, group_read_vectors, head_filter_taps.shape[0]
    )
    tp_count = lax.axis_size("tp")
    ep_count = lax.axis_size("ep")
    tok_local = expert_input_rows.shape[0]
    model_width = expert_input_rows.shape[1]
    top_count = routes.shape[1]
    local_experts = routed_gate_weight.shape[0]
    experts = local_experts * ep_count
    capacity = 3 * tok_local * top_count // (2 * experts)
    rows_float = expert_input_rows.astype(jnp.float32)
    normed = (
        rows_float
        * lax.rsqrt(jnp.mean(rows_float * rows_float, axis=-1, keepdims=True) + eps_norm)
        * expert_norm_gain
    ).astype(jnp.bfloat16)
    score_float = router_chosen_scores.astype(jnp.float32)
    weights = score_float / jnp.sum(score_float, axis=1, keepdims=True) * route_scale
    choice = routes[None, :, :] == jnp.arange(experts, dtype=jnp.int32)[:, None, None]
    named = jnp.any(choice, axis=2)
    weight_of = jnp.sum(jnp.where(choice, weights[None], 0.0), axis=2)
    row_order = jnp.arange(tok_local, dtype=jnp.int32)
    earlier_rows = (row_order[:, None] < row_order[None, :]).astype(jnp.bfloat16)
    rank = jnp.dot(
        named.astype(jnp.bfloat16), earlier_rows, preferred_element_type=jnp.float32
    ).astype(jnp.int32)

    cuts = [0, capacity // 2, capacity] if capacity > 1 else [0, capacity]
    picks, outgoing = [], []
    for low, high in zip(cuts[:-1], cuts[1:]):
        places = jnp.arange(low, high, dtype=jnp.int32)
        picked = named[:, None, :] & (rank[:, None, :] == places[None, :, None])
        picks.append(picked)
        outgoing.append(
            jnp.dot(
                picked.reshape(-1, tok_local).astype(jnp.bfloat16),
                normed,
                preferred_element_type=jnp.float32,
            ).astype(jnp.bfloat16)
        )
    earlier, outgoing[0] = lax.optimization_barrier((earlier, outgoing[0]))
    group_rows = lax.all_gather(normed, "tp", axis=0, tiled=True)

    arrived = []
    for block in outgoing:
        arrived.append(lax.all_to_all(block, "ep", split_axis=0, concat_axis=0, tiled=True))
    gathered = [lax.all_gather(block, "tp", axis=0) for block in arrived]

    shared_hidden = (
        jax.nn.silu(jnp.dot(group_rows, shared_gate_weight, preferred_element_type=jnp.float32))
        * jnp.dot(group_rows, shared_up_weight, preferred_element_type=jnp.float32)
    ).astype(jnp.bfloat16)
    shared_part = jnp.dot(shared_hidden, shared_down_weight, preferred_element_type=jnp.float32)

    mixer_normed = mixer_rows(
        earlier,
        head_inputs_unfiltered,
        group_write_vectors,
        group_read_vectors,
        output_gate_inputs,
        step_preactivation,
        extra_decay_logs,
        head_decay_logs,
        head_filter_taps,
        write_filter_taps,
        read_filter_taps,
        grouped_norm_gain,
    )

    def expert_rows(block):
        sources = block.reshape(tp_count, ep_count, local_experts, -1, model_width)
        gate_value = jnp.einsum(
            "osecd,edf->osecf", sources, routed_gate_weight, preferred_element_type=jnp.float32
        )
        up_value = jnp.einsum(
            "osecd,edf->osecf", sources, routed_up_weight, preferred_element_type=jnp.float32
        )
        hidden = (jax.nn.silu(gate_value) * up_value).astype(jnp.bfloat16)
        partial_value = jnp.einsum(
            "osecf,efd->osecd", hidden, routed_down_weight, preferred_element_type=jnp.float32
        ).astype(jnp.bfloat16)
        return lax.psum_scatter(
            partial_value.reshape(-1, model_width), "tp", scatter_dimension=0, tiled=True
        )

    own_term = jnp.zeros((tok_local, model_width), jnp.float32)
    for block, picked in zip(gathered, picks):
        returned = lax.all_to_all(
            expert_rows(block), "ep", split_axis=0, concat_axis=0, tiled=True
        )
        mixing = jnp.where(picked, weight_of[:, None, :], 0.0).reshape(-1, tok_local)
        own_term = own_term + jnp.einsum(
            "sr,sd->rd", mixing, returned.astype(jnp.float32), precision=highest
        )
    mix_block = mixer_normed.shape[0] // tp_count
    block_rows = mix_block + tok_local
    mix_term = jnp.dot(
        mixer_normed, mixer_output_weight, preferred_element_type=jnp.float32
    ).astype(jnp.bfloat16).reshape(tp_count, mix_block, model_width)
    moe_term = shared_part.astype(jnp.bfloat16).reshape(tp_count, tok_local, model_width)
    row_sums = lax.psum_scatter(
        jnp.concatenate([mix_term, moe_term], axis=1).reshape(tp_count * block_rows, model_width),
        "tp",
        scatter_dimension=0,
        tiled=True,
    )
    mixer_result = row_sums[:mix_block]
    moe_total = row_sums[mix_block:].astype(jnp.float32) + own_term
    return (mixer_result.astype(jnp.bfloat16), moe_total.astype(jnp.bfloat16))


def solution(mesh):
    in_specs = (
        P("ep", "tp"),
        P("ep", "tp"),
        P("ep", "tp"),
        P("ep", "tp"),
        P("tp", "ep"),
        P("tp", "ep"),
        P("tp"),
        P(None, "tp"),
        P(None, "tp"),
        P(None, "tp"),
        P("tp"),
        P("tp", None),
        P(("ep", "tp"), None),
        P(),
        P(("ep", "tp"), None),
        P(("ep", "tp"), None),
        P("ep", None, "tp"),
        P("ep", None, "tp"),
        P("ep", "tp", None),
        P(None, "tp"),
        P(None, "tp"),
        P("tp", None),
    )
    out_specs = (P(("ep", "tp"), None), P(("ep", "tp"), None))
    return jax.shard_map(local, mesh=mesh, in_specs=in_specs, out_specs=out_specs, check_vma=False)
```

time: 393 us -> 302 us (0.77)
  waiting for transfers between devices: 227 us -> 146 us
  local copies, waits for them, and re-layouts: 32.5 us -> 8.93 us
  blocking collectives: 33.9 us -> 50.5 us
  other arithmetic: 26.8 us -> 14.6 us
  matrix products: 42 us -> 51.3 us
    all_to_all x2, waiting for transfers between devices: 105 us -> 0.01 us  [local(): lax.all_to_all(expert_rows(block), 'ep', split_axis=0, concat_axis=0, til...]
    all_to_all x0 -> x2, blocking collectives: none -> 50.5 us  [local(): lax.all_to_all(block, 'ep', split_axis=0, concat_axis=0, tiled=True)]
    reduce_scatter x2 -> x3, waiting for transfers between devices: 36.1 us -> 84 us  [the longest x2 52.5 us: expert_rows(): lax.psum_scatter(partial_value.reshape(-1, model_width), 'tp', scatter_di...]
    ppermute x1, waiting for transfers between devices: 46.1 us -> 0.98 us  [from_behind(): return lax.ppermute(value, axis, pairs)]
    all_gather x3 -> x0, blocking collectives: 33.9 us -> none  [the longest x1 22.3 us: carried_in(): pieces = jax.tree.map(lambda part: lax.all_gather(part, axis), value)]
    all_gather x2 -> x4, waiting for transfers between devices: 39.9 us -> 60.4 us  [the longest x1 43.6 us: carried_in(): pieces = lax.all_gather(packed, axis).astype(jnp.float32)]
    gather x2 -> x0, local copies, waits for them, and re-layouts: 9.81 us -> none  [the longest x1 7.11 us: local(): padded_rows[slot_token].reshape(tp_count, experts, capacity, model_width)]
    dot_general x2 -> x9, matrix products: 18.6 us -> 27.8 us  [the longest x2 15 us: expert_rows(): jnp.einsum('osecf,efd->osecd', hidden, routed_down_weight, preferred_elem...]
  transfers between devices with their start and end apart: 7 -> 10, of which waited for: 6 -> 7; matrix products, arithmetic and copies ran while one was open for 18% -> 22% of each run, Pallas kernels for 0% -> 0%
where the time goes in v1:
time: 302 us; the launch traced here: 301 us
  waiting for transfers between devices  146 us (48%)
  matrix products  51.3 us (17%)
  blocking collectives  50.5 us (17%)
  starting transfers between devices  14.9 us (5%)
  between operations  14.8 us (5%)
  other arithmetic  14.6 us (5%)
  local copies, waits for them, and re-layouts  8.93 us (3%)
    reduce_scatter x2, waiting for transfers between devices, expert_rows(): lax.psum_scatter(partial_value.reshape(-1, model_width), 'tp', scatter_di...  52.5 us
    all_to_all x2, blocking collectives, local(): lax.all_to_all(block, 'ep', split_axis=0, concat_axis=0, tiled=True)  50.5 us
    all_gather x1, waiting for transfers between devices, carried_in(): pieces = lax.all_gather(packed, axis).astype(jnp.float32)  43.6 us
    reduce_scatter x1, waiting for transfers between devices, local(): lax.psum_scatter(jnp.concatenate([mix_term, moe_term], axis=1).reshape(tp...  31.5 us
    dot_general x2, matrix products, expert_rows(): jnp.einsum('osecf,efd->osecd', hidden, routed_down_weight, preferred_elem...  15 us
    all_to_all x2, starting transfers between devices, local(): lax.all_to_all(expert_rows(block), 'ep', split_axis=0, concat_axis=0, til...  11.1 us
    all_gather x2, waiting for transfers between devices, local(): gathered = [lax.all_gather(block, 'tp', axis=0) for block in arrived]  8.59 us
    dot_general x2, matrix products, expert_rows(): jnp.einsum('osecd,edf->osecf', sources, routed_gate_weight, preferred_ele...  8.56 us
  transfers between devices with their start and end apart: 10, of which 7 were waited for; matrix products, arithmetic and copies ran while one was open for 22% of the time, Pallas kernels for 0%

profile of v1, /device:TPU:0, one launch (start us, length us, event | category | flops | bytes accessed | tf_op | source)
XLA Modules:
  0.0 301.1 jit_solution(403880158570030058)
XLA Ops:
  7.3 0.8 fusion.104
  8.4 1.2 fusion.15
  9.6 1.2 fusion.17
  11.0 0.4 convolution_convert_fusion.3
  11.4 27.5 %all_to_all.36 = bf16[8,24,2048]{2,1,0:T(8,128)(2,1)} all-to-all(bf16[8,24,2048]{2,1,0:T(8,128)(2,1)S(1)} %bitcast.259), channel_id=1, replica_groups=mesh['ep'=8,'tp'=4] {'ep'}, dimensions={0} | all-to-all | bytes 1572864 | tf_op jit(solution)/shard_map/all_to_all | solution.py:219
  39.1 3.3 %collective-permute-start = (bf16[3,1280]{1,0:T(4,128)(2,1)S(1)}, bf16[3,1280]{1,0:T(4,128)(2,1)S(1)}, u32[]{:S(2)}, u32[]{:S(2)}) collective-permute-start(bf16[3,1280]{1,0:T(4,128)(2,1)S(1)} %pad_maximum_fusion.5), channel_id=1, source_target_pairs={{0,4},{4,8},{8,12},{12,16},{16,20},{20,24},{24,28},{1,5},{5,9},{9,... | collective-permute-start | bytes 23048 | tf_op jit(solution)/shard_map/ppermute | solution.py:19
  42.4 0.4 convolution_convert_fusion.4
  42.8 1.0 collective-permute-done
  43.8 23.0 %all_to_all.37 = bf16[8,24,2048]{2,1,0:T(8,128)(2,1)} all-to-all(bf16[8,24,2048]{2,1,0:T(8,128)(2,1)S(1)} %bitcast.258), channel_id=1, replica_groups=mesh['ep'=8,'tp'=4] {'ep'}, dimensions={0} | all-to-all | bytes 1572864 | tf_op jit(solution)/shard_map/all_to_all | solution.py:219
  66.8 0.7 all-gather.7.cloned.1.call-update
  67.8 0.5 reduce_window_sum.24
  69.5 0.4 copy.63
  70.1 1.1 fusion.26
  71.2 3.8 %fusion.34 = f32[16,1,64,128]{3,1,2,0:T(1,128)S(1)} fusion(f32[16,2,1,1]{1,2,3,0:T(1,128)S(1)} %copy.75, f32[2,16,64,128]{3,2,1,0:T(8,128)S(1)} %fusion.26), kind=kOutput, calls=%fused_computation.54 | convolution fusion | flops 3145728 | bytes 1572992 | tf_op jit(solution)/shard_map/gec,cgepn->gepn/dot_general | solution.py:124
  75.1 0.7 pad_maximum_fusion.1
  75.9 4.5 %convolution_bitcast_fusion.6 = f32[4,8,1,24,256]{4,3,1,0,2:T(8,128)} fusion(bf16[4,8,24,2048]{3,2,1,0:T(8,128)(2,1)} %bitcast.280, bf16[1,2048,256]{2,1,0:T(8,128)(2,1)} %param.38), kind=kOutput, calls=%fused_computation.22 | convolution fusion | flops 805306368 | bytes 4980736 | tf_op jit(solution)/shard_map/osecd,edf->osecf/dot_general | solution.py:245
  80.4 7.5 %convolution_convert_fusion = bf16[4,8,24,2048]{3,2,1,0:T(8,128)(2,1)} fusion(bf16[4,8,24,2048]{3,2,1,0:T(8,128)(2,1)} %bitcast.281, bf16[1,256,2048]{2,1,0:T(8,128)(2,1)S(1)} %copy-done, bf16[1,2048,256]{2,1,0:T(8,128)(2,1)} %param.39, f32[4,8,1,24,256]{4,3,1,0,2:T(8,128)} %convolution_bitcast_fusion.6), kind=kOutput, calls=%fused_computation.2 | convolution fusion | flops 1613365248 | bytes 9175040 | tf_op jit(solution)/shard_map/osecf,efd->osecd/dot_general | solution.py:252
  88.2 8.6 %all-gather.9.cloned.1.call-done = bf16[4,192,2048]{2,1,0:T(8,128)(2,1)} async-done(((bf16[1,192,2048]{2,1,0:T(8,128)(2,1)}), bf16[4,192,2048]{2,1,0:T(8,128)(2,1)}) %all-gather.9.cloned.1.call-update) | async-done | bytes 3145744 | tf_op jit(solution)/shard_map/all_gather | solution.py:220
  96.8 4.0 %convolution_bitcast_fusion.8 = f32[4,8,1,24,256]{4,3,1,0,2:T(8,128)} fusion(bf16[4,8,24,2048]{3,2,1,0:T(8,128)(2,1)} %bitcast.282, bf16[1,2048,256]{2,1,0:T(8,128)(2,1)} %param.38), kind=kOutput, calls=%fused_computation.24 | convolution fusion | flops 805306368 | bytes 4980736 | tf_op jit(solution)/shard_map/osecd,edf->osecf/dot_general | solution.py:245
  100.8 7.5 %convolution_convert_fusion.1 = bf16[4,8,24,2048]{3,2,1,0:T(8,128)(2,1)} fusion(bf16[4,8,24,2048]{3,2,1,0:T(8,128)(2,1)} %bitcast.283, bf16[1,256,2048]{2,1,0:T(8,128)(2,1)S(1)} %copy-done, bf16[1,2048,256]{2,1,0:T(8,128)(2,1)} %param.39, f32[4,8,1,24,256]{4,3,1,0,2:T(8,128)} %convolution_bitcast_fusion.8), kind=kOutput, calls=%fused_computation.3 | convolution fusion | flops 1613365248 | bytes 9175040 | tf_op jit(solution)/shard_map/osecf,efd->osecd/dot_general | solution.py:252
  108.4 0.7 copy.69
  109.2 0.8 copy.81
  110.0 0.7 copy.67
  110.7 0.6 iota_compare_fusion.4
  111.3 0.6 iota_compare_fusion.7
  111.9 0.6 fusion.105
  112.5 0.6 exponential_bitcast_fusion
  113.4 8.1 %all-gather.7.cloned.1.call-done = bf16[512,2048]{1,0:T(8,128)(2,1)} async-done(((bf16[128,2048]{1,0:T(8,128)(2,1)}), bf16[512,2048]{1,0:T(8,128)(2,1)}) %all-gather.7.cloned.1.call-update) | async-done | bytes 2097168 | tf_op jit(solution)/shard_map/all_gather | solution.py:215
  121.5 2.4 fusion.119
  123.9 5.5 %convolution_convert_fusion.2 = bf16[512,2048]{1,0:T(8,128)(2,1)} fusion(bf16[128,2048]{1,0:T(8,128)(2,1)} %param.43, bf16[512,2048]{1,0:T(8,128)(2,1)} %all-gather.7.cloned.1.call-done, bf16[2048,128]{1,0:T(8,128)(2,1)} %param.42, f32[512,128]{1,0:T(8,128)S(1)} %fusion.119), kind=kOutput, calls=%fused_computation.4 | convolution fusion | flops 538312704 | bytes 5505024 | tf_op jit(solution)/shard_map/dot_general | solution.py:226
  129.4 43.6 %all-gather.5.cloned.1.call-done = bf16[8,1040,128]{2,1,0:T(8,128)(2,1)} async-done(((bf16[1,1040,128]{2,1,0:T(8,128)(2,1)}), bf16[8,1040,128]{2,1,0:T(8,128)(2,1)}) %all-gather.5.cloned.1.call-update) | async-done | bytes 2129936 | tf_op jit(solution)/shard_map/all_gather | solution.py:34
  173.0 1.9 convert_element_type.164
  174.9 2.0 copy-done.1
  177.4 3.2 %fusion = f32[1024,128]{1,0:T(8,128)S(1)} fusion(f32[8,1040,128]{2,1,0:T(8,128)} %copy-done.1, f32[8,1024]{1,0:T(8,128)S(1)} %mul.387), kind=kLoop, calls=%fused_computation.1 | loop fusion | flops 1966080 | bytes 4751360 | tf_op jit(solution)/shard_map/reduce_sum | solution.py:41
  180.6 4.2 %fusion.11 = f32[2,16,64,128]{3,0,2,1:T(2,128)S(1)} fusion(f32[2,16,64,128]{3,2,1,0:T(8,128)S(1)} %fusion.26, f32[16,64,128]{2,1,0:T(8,128)S(1)} %bitcast.268, f32[2,16]{0,1:T(8,128)S(1)} %copy-done.18, pred[2,2]{1,0:T(4,128)(4,1)S(1)} %copy-done.33, f32[16,2]{1,0:T(8,128)S(1)} %copy-done.19, f32[16,2]{1,0:T(8,128)S(1)} %bitcast.279), kind=kOutput, calls=%fused_computation.30 | convolution fusion | flops 6815872 | bytes 2621828 | tf_op jit(solution)/shard_map/gebc,cgepn->bgepn/dot_general | solution.py:122
  184.9 1.0 fusion.5
  185.9 2.0 fusion.4
  188.0 0.5 copy.72
  189.1 3.2 %convolution_convert_fusion.5 = bf16[128,2048]{1,0:T(8,128)(2,1)S(1)} fusion(bf16[1024,2048]{1,0:T(8,128)(2,1)} %param.33, f32[1024]{0:T(1024)S(1)} %copy-done.31, f32[128]{0:T(128)S(1)} %add_rsqrt_fusion, f32[128,1024]{1,0:T(8,128)S(1)} %reshape.391, bf16[128,1024]{1,0:T(8,128)(2,1)S(1)} %copy-done.5), kind=kOutput, calls=%fused_computation.13 | convolution fusion | flops 538312704 | bytes 5509632 | tf_op jit(solution)/shard_map/dot_general | solution.py:270
  192.3 1.8 pad_maximum_fusion
  194.1 17.7 %reduce-scatter.8.cloned.1.call-done = bf16[192,2048]{1,0:T(8,128)(2,1)} async-done(((bf16[768,2048]{1,0:T(8,128)(2,1)}), bf16[192,2048]{1,0:T(8,128)(2,1)}) %reduce-scatter.8.cloned.1.call-update) | async-done | bytes 786448 | tf_op jit(solution)/shard_map/reduce_scatter | solution.py:255
  211.8 5.5 %all-to-all-start.3 = ((bf16[8,24,2048]{2,1,0:T(8,128)(2,1)}), bf16[8,24,2048]{2,1,0:T(8,128)(2,1)S(1)}, u32[]{:S(2)}, u32[]{:S(2)}) async-start(bf16[8,24,2048]{2,1,0:T(8,128)(2,1)} %bitcast.263), calls=%async_computation.6 | async-start | bytes 1572864 | tf_op jit(solution)/shard_map/all_to_all | solution.py:261
  217.4 34.8 %reduce-scatter.6.cloned.1.call-done = bf16[192,2048]{1,0:T(8,128)(2,1)} async-done(((bf16[768,2048]{1,0:T(8,128)(2,1)}), bf16[192,2048]{1,0:T(8,128)(2,1)}) %reduce-scatter.6.cloned.1.call-update) | async-done | bytes 786448 | tf_op jit(solution)/shard_map/reduce_scatter | solution.py:255
  252.1 5.5 %all-to-all-start.1 = ((bf16[8,24,2048]{2,1,0:T(8,128)(2,1)}), bf16[8,24,2048]{2,1,0:T(8,128)(2,1)}, u32[]{:S(2)}, u32[]{:S(2)}) async-start(bf16[8,24,2048]{2,1,0:T(8,128)(2,1)} %bitcast.262), calls=%async_computation.3 | async-start | bytes 1572864 | tf_op jit(solution)/shard_map/all_to_all | solution.py:261
  257.7 31.5 %reduce-scatter.4.cloned.1.call-done = bf16[160,2048]{1,0:T(8,128)(2,1)} async-done(((bf16[640,2048]{1,0:T(8,128)(2,1)}), bf16[160,2048]{1,0:T(8,128)(2,1)}) %reduce-scatter.4.cloned.1.call-update) | async-done | bytes 655376 | tf_op jit(solution)/shard_map/reduce_scatter | solution.py:274
  289.2 1.6 slice.148
  290.8 0.7 convolution_bitcast_fusion
  291.5 2.7 fusion.3
  (136 shorter events, 4.2 us)
Async XLA Ops:
  7.2 73.3 %copy-start = (bf16[1,256,2048]{2,1,0:T(8,128)(2,1)S(1)}, bf16[1,256,2048]{2,1,0:T(8,128)(2,1)}, u32[]{:S(2)}) copy-start(bf16[1,256,2048]{2,1,0:T(8,128)(2,1)} %param.40) | copy-start | bytes 3145732
  7.2 31.8 %copy-start.4 = (bf16[128,1024]{1,0:T(8,128)(2,1)S(1)}, bf16[128,1024]{1,0:T(8,128)(2,1)}, u32[]{:S(2)}) copy-start(bf16[128,1024]{1,0:T(8,128)(2,1)} %param.22) | copy-start | bytes 786436
  7.2 31.8 %copy-start.11 = (bf16[128,128]{1,0:T(8,128)(2,1)S(1)}, bf16[128,128]{1,0:T(8,128)(2,1)}, u32[]{:S(2)}) copy-start(bf16[128,128]{1,0:T(8,128)(2,1)} %param.23) | copy-start | bytes 98308
  7.2 31.8 %copy-start.12 = (bf16[128,128]{1,0:T(8,128)(2,1)S(1)}, bf16[128,128]{1,0:T(8,128)(2,1)}, u32[]{:S(2)}) copy-start(bf16[128,128]{1,0:T(8,128)(2,1)} %param.24) | copy-start | bytes 98308
  7.2 68.7 %all-gather.11.cloned.1.call-start = ((), (), s32[]{:S(2)}) async-start(), calls=%async_computation.12 | async-start | bytes 3932160 | tf_op jit(solution)/shard_map/all_gather | solution.py:220
  7.3 3.6 %copy-start.25 = (s32[24]{0:T(128)}, s32[24]{0:T(128)S(1)}, u32[]{:S(2)}) copy-start(s32[24]{0:T(128)S(1)} %iota_add_fusion) | copy-start | bytes 292
  8.0 34.7 %copy-start.15 = (pred[8,128]{1,0:T(8,128)(4,1)}, pred[8,128]{1,0:T(8,128)(4,1)S(1)}, u32[]{:S(2)}) copy-start(pred[8,128]{1,0:T(8,128)(4,1)S(1)} %fusion.104) | copy-start | bytes 3076
  8.2 34.6 %copy-start.9 = (s32[8,128]{1,0:T(8,128)}, s32[8,128]{1,0:T(8,128)S(1)}, u32[]{:S(2)}) copy-start(s32[8,128]{1,0:T(8,128)S(1)} %convolution_convert_fusion.6) | copy-start | bytes 12292
  10.8 55.9 %copy-start.3 = (bf16[128,2048]{1,0:T(8,128)(2,1)}, bf16[128,2048]{1,0:T(8,128)(2,1)S(1)}, u32[]{:S(2)}) copy-start(bf16[128,2048]{1,0:T(8,128)(2,1)S(1)} %fusion.17) | copy-start | bytes 1572868
  11.4 56.2 %copy-start.32 = (f32[16]{0:T(128)S(1)}, f32[16]{0:T(128)}, u32[]{:S(2)}) copy-start(f32[16]{0:T(128)} %param.28) | copy-start | bytes 196
  11.4 56.2 %copy-start.20 = (f32[16,128]{1,0:T(8,128)S(1)}, f32[16,128]{1,0:T(8,128)}, u32[]{:S(2)}) copy-start(f32[16,128]{1,0:T(8,128)} %param.26) | copy-start | bytes 24580
  11.4 56.2 %copy-start.21 = (f32[16,128]{1,0:T(8,128)S(1)}, f32[16,128]{1,0:T(8,128)}, u32[]{:S(2)}) copy-start(f32[16,128]{1,0:T(8,128)} %param.27) | copy-start | bytes 24580
  11.4 57.3 %copy-start.22 = (bf16[4,128]{1,0:T(4,128)(2,1)S(1)}, bf16[4,128]{1,0:T(4,128)(2,1)}, u32[]{:S(2)}) copy-start(bf16[4,128]{1,0:T(4,128)(2,1)} %param.30) | copy-start | bytes 3076
  11.4 57.4 %copy-start.23 = (bf16[4,128]{1,0:T(4,128)(2,1)S(1)}, bf16[4,128]{1,0:T(4,128)(2,1)}, u32[]{:S(2)}) copy-start(bf16[4,128]{1,0:T(4,128)(2,1)} %param.31) | copy-start | bytes 3076
  11.4 57.4 %copy-start.14 = (bf16[4,1024]{1,0:T(4,128)(2,1)S(1)}, bf16[4,1024]{1,0:T(4,128)(2,1)}, u32[]{:S(2)}) copy-start(bf16[4,1024]{1,0:T(4,128)(2,1)} %param.29) | copy-start | bytes 24580
  38.9 57.8 %all-gather.9.cloned.1.call-start = ((), (), s32[]{:S(2)}) async-start(), calls=%async_computation.10 | async-start | bytes 3932160 | tf_op jit(solution)/shard_map/all_gather | solution.py:220
  39.1 4.7 %collective-permute-start = (bf16[3,1280]{1,0:T(4,128)(2,1)S(1)}, bf16[3,1280]{1,0:T(4,128)(2,1)S(1)}, u32[]{:S(2)}, u32[]{:S(2)}) collective-permute-start(bf16[3,1280]{1,0:T(4,128)(2,1)S(1)} %pad_maximum_fusion.5), channel_id=1, source_target_pairs={{0,4},{4,8},{8,12},{12,16},{16,20},{20,24},{24,28},{1,5},{5,9},{9,... | collective-permute-start | bytes 23048 | tf_op jit(solution)/shard_map/ppermute | solution.py:19
  66.8 54.7 %all-gather.7.cloned.1.call-start = ((), (), s32[]{:S(2)}) async-start(), calls=%async_computation.8 | async-start | bytes 2621440 | tf_op jit(solution)/shard_map/all_gather | solution.py:215
  67.5 105.5 %all-gather.5.cloned.1.call-start = ((), (), s32[]{:S(2)}) async-start(), calls=%async_computation.7 | async-start | bytes 2396160 | tf_op jit(solution)/shard_map/all_gather | solution.py:34
  68.5 2.7 copy-start.6
  75.8 136.0 %reduce-scatter.8.cloned.1.call-start = ((), (), s32[]{:S(2)}) async-start(), calls=%async_computation.13 | async-start | bytes 3932160 | tf_op jit(solution)/shard_map/reduce_scatter | solution.py:255
  88.0 164.2 %reduce-scatter.6.cloned.1.call-start = ((), (), s32[]{:S(2)}) async-start(), calls=%async_computation.11 | async-start | bytes 3932160 | tf_op jit(solution)/shard_map/reduce_scatter | solution.py:255
  108.3 180.9 %reduce-scatter.4.cloned.1.call-start = ((), (), s32[]{:S(2)}) async-start(), calls=%async_computation.9 | async-start | bytes 3276800 | tf_op jit(solution)/shard_map/reduce_scatter | solution.py:274
  110.7 2.7 copy-start.28
  129.4 47.6 %copy-start.27 = (pred[8,8]{1,0:T(8,128)(4,1)S(1)}, pred[8,8]{1,0:T(8,128)(4,1)}, u32[]{:S(2)}) copy-start(pred[8,8]{1,0:T(8,128)(4,1)} %fusion.105) | copy-start | bytes 196
  129.4 47.7 %copy-start.29 = (pred[8]{0:T(512)(128)(4,1)S(1)}, pred[8]{0:T(512)(128)(4,1)}, u32[]{:S(2)}) copy-start(pred[8]{0:T(512)(128)(4,1)} %copy-done.28) | copy-start | bytes 28
  174.9 2.0 copy-start.1
  176.9 3.7 %copy-start.17 = (f32[1,16,2,1]{2,1,3,0:T(8,128)S(1)}, f32[1,16,2,1]{2,1,3,0:T(8,128)}, u32[]{:S(2)}) copy-start(f32[1,16,2,1]{2,1,3,0:T(8,128)} %copy.81) | copy-start | bytes 388
  176.9 3.7 %copy-start.18 = (f32[2,16]{0,1:T(8,128)S(1)}, f32[2,16]{0,1:T(8,128)}, u32[]{:S(2)}) copy-start(f32[2,16]{0,1:T(8,128)} %copy.69) | copy-start | bytes 388
  176.9 3.7 %copy-start.19 = (f32[16,2]{1,0:T(8,128)S(1)}, f32[16,2]{1,0:T(8,128)}, u32[]{:S(2)}) copy-start(f32[16,2]{1,0:T(8,128)} %copy.67) | copy-start | bytes 388
  176.9 3.7 %copy-start.33 = (pred[2,2]{1,0:T(4,128)(4,1)S(1)}, pred[2,2]{1,0:T(4,128)(4,1)}, u32[]{:S(2)}) copy-start(pred[2,2]{1,0:T(4,128)(4,1)} %iota_compare_fusion.7) | copy-start | bytes 16
  180.5 4.3 %copy-start.8 = (f32[2,64,16]{1,2,0:T(8,128)S(1)}, f32[2,64,16]{1,2,0:T(8,128)}, u32[]{:S(2)}) copy-start(f32[2,64,16]{1,2,0:T(8,128)} %exponential_bitcast_fusion) | copy-start | bytes 24580
  180.5 5.3 %copy-start.7 = (f32[2,64,16]{1,2,0:T(8,128)S(1)}, f32[2,64,16]{1,2,0:T(8,128)}, u32[]{:S(2)}) copy-start(f32[2,64,16]{1,2,0:T(8,128)} %copy-done.6) | copy-start | bytes 24580
  180.6 5.3 %copy-start.13 = (pred[64,64]{1,0:T(8,128)(4,1)S(1)}, pred[64,64]{1,0:T(8,128)(4,1)}, u32[]{:S(2)}) copy-start(pred[64,64]{1,0:T(8,128)(4,1)} %iota_compare_fusion.4) | copy-start | bytes 12292
  185.9 2.9 copy-start.5
  185.9 3.2 %copy-start.31 = (f32[1024]{0:T(1024)S(1)}, f32[1024]{0:T(1024)}, u32[]{:S(2)}) copy-start(f32[1024]{0:T(1024)} %param.32) | copy-start | bytes 12292
  189.1 3.2 %copy-start.2 = (bf16[512,2048]{1,0:T(8,128)(2,1)S(1)}, bf16[512,2048]{1,0:T(8,128)(2,1)}, u32[]{:S(2)}) copy-start(bf16[512,2048]{1,0:T(8,128)(2,1)} %convolution_convert_fusion.2) | copy-start | bytes 6291460
  194.0 63.6 %copy-start.30 = (bf16[128,2]{0,1:T(2,128)(2,1)S(1)}, bf16[128,2]{0,1:T(2,128)(2,1)}, u32[]{:S(2)}) copy-start(bf16[128,2]{0,1:T(2,128)(2,1)} %param.37) | copy-start | bytes 1540
  194.0 63.7 %copy-start.24 = (s32[128,2]{0,1:T(2,128)S(1)}, s32[128,2]{0,1:T(2,128)}, u32[]{:S(2)}) copy-start(s32[128,2]{0,1:T(2,128)} %param.36) | copy-start | bytes 3076
  194.0 96.8 %copy-start.10 = (s32[8,128]{1,0:T(8,128)S(1)}, s32[8,128]{1,0:T(8,128)}, u32[]{:S(2)}) copy-start(s32[8,128]{1,0:T(8,128)} %copy-done.9) | copy-start | bytes 12292
  194.0 96.8 %copy-start.16 = (pred[8,128]{1,0:T(8,128)(4,1)S(1)}, pred[8,128]{1,0:T(8,128)(4,1)}, u32[]{:S(2)}) copy-start(pred[8,128]{1,0:T(8,128)(4,1)} %copy-done.15) | copy-start | bytes 3076
  194.1 96.8 %copy-start.26 = (s32[24]{0:T(128)S(1)}, s32[24]{0:T(128)}, u32[]{:S(2)}) copy-start(s32[24]{0:T(128)} %copy-done.25) | copy-start | bytes 292
  211.8 40.3 %all-to-all-start.3 = ((bf16[8,24,2048]{2,1,0:T(8,128)(2,1)}), bf16[8,24,2048]{2,1,0:T(8,128)(2,1)S(1)}, u32[]{:S(2)}, u32[]{:S(2)}) async-start(bf16[8,24,2048]{2,1,0:T(8,128)(2,1)} %bitcast.263), calls=%async_computation.6 | async-start | bytes 1572864 | tf_op jit(solution)/shard_map/all_to_all | solution.py:261
  252.1 39.4 %all-to-all-start.1 = ((bf16[8,24,2048]{2,1,0:T(8,128)(2,1)}), bf16[8,24,2048]{2,1,0:T(8,128)(2,1)}, u32[]{:S(2)}, u32[]{:S(2)}) async-start(bf16[8,24,2048]{2,1,0:T(8,128)(2,1)} %bitcast.262), calls=%async_computation.3 | async-start | bytes 1572864 | tf_op jit(solution)/shard_map/all_to_all | solution.py:261
Sparse Core Ops, SparseCore 0:
  39.0 27.5 all-gather.10
  68.2 28.5 all-gather.8
  98.9 22.5 all-gather.6
  123.5 49.4 all-gather.4
  175.4 36.3 reduce-scatter.7
  214.2 37.8 reduce-scatter.5
  254.7 34.5 reduce-scatter.3

commit v2 on v1

--- a/solution.py
+++ b/solution.py
@@ -19,26 +19,38 @@
     return lax.ppermute(value, axis, pairs)
 
 
-def carried_in(decay, state, axis):
-    count, mine = (lax.axis_size(axis), lax.axis_index(axis))
-    heads = decay.size
-    width = state.shape[-1]
-    flat_decay = decay.reshape(heads)
-    parts, rest = [], flat_decay
+def sent_state(decay, state, axis, by):
+    heads, width = decay.shape[0], state.shape[-1]
+    parts, rest = [], decay
     for _ in range(3):
         part = lax.reduce_precision(rest, exponent_bits=8, mantissa_bits=7)
         parts.append(part)
         rest = rest - part
     decay_rows = jnp.pad(jnp.stack(parts, axis=1), ((0, 0), (0, width - 3)))
     packed = jnp.concatenate([state.reshape(-1, width), decay_rows], axis=0).astype(jnp.bfloat16)
-    pieces = lax.all_gather(packed, axis).astype(jnp.float32)
-    decays = jnp.sum(pieces[:, -heads:, :3], axis=-1)
-    order = jnp.arange(count, dtype=jnp.int32)
-    between = (order[None, :] > order[:, None]) & (order[None, :] < mine)
-    spans = jnp.sum(jnp.where(between[:, :, None], decays[None], 0.0), axis=1)
-    ratio = jnp.where((order < mine)[:, None], jnp.exp(spans), 0.0)
-    states = pieces[:, :-heads].reshape((count, heads) + state.shape[-2:])
-    return jnp.sum(states * ratio[:, :, None, None], axis=0).reshape(state.shape)
+    packed = from_behind(packed, axis, by).astype(jnp.float32)
+    return jnp.sum(packed[-heads:, :3], axis=-1), packed[:-heads].reshape(state.shape)
+
+
+def carried_in(decay, state, axis):
+    shape = state.shape
+    own = (decay.reshape(-1), state.reshape((-1,) + shape[-2:]))
+    before, by = None, 1
+    while by < lax.axis_size(axis):
+        span = own if before is None else combine_states(before, own)
+        received = sent_state(*span, axis, by)
+        before = received if before is None else combine_states(received, before)
+        by *= 2
+    if before is None:
+        return jnp.zeros_like(state)
+    return before[1].reshape(shape)
+
+
+def combine_states(earlier_part, later_part):
+    return (
+        earlier_part[0] + later_part[0],
+        later_part[1] + jnp.exp(later_part[0])[..., None, None] * earlier_part[1],
+    )
 
 
 def conv_silu(values, weights):
@@ -211,8 +223,8 @@
                 preferred_element_type=jnp.float32,
             ).astype(jnp.bfloat16)
         )
-    earlier, outgoing[0] = lax.optimization_barrier((earlier, outgoing[0]))
     group_rows = lax.all_gather(normed, "tp", axis=0, tiled=True)
+    earlier, group_rows, outgoing[0] = lax.optimization_barrier((earlier, group_rows, outgoing[0]))
 
     arrived = []
     for block in outgoing:

time: 302 us -> 233 us (0.77)
  waiting for transfers between devices: 146 us -> 35.4 us
  blocking collectives: 50.5 us -> 80.4 us
  starting transfers between devices: 14.9 us -> 22.3 us
  matrix products: 51.3 us -> 57.2 us
    reduce_scatter x2, waiting for transfers between devices: 52.5 us -> 0.02 us  [expert_rows(): lax.psum_scatter(partial_value.reshape(-1, model_width), 'tp', scatter_di...]
    all_gather x1 -> x0, waiting for transfers between devices: 43.6 us -> none  [carried_in(): pieces = lax.all_gather(packed, axis).astype(jnp.float32)]
    all_to_all x0 -> x1, blocking collectives: none -> 30 us  [local(): lax.all_to_all(expert_rows(block), 'ep', split_axis=0, concat_axis=0, til...]
    reduce_scatter x1, waiting for transfers between devices: 31.5 us -> 13.4 us  [local(): lax.psum_scatter(jnp.concatenate([mix_term, moe_term], axis=1).reshape(tp...]
    ppermute x1 -> x4, starting transfers between devices: 3.33 us -> 18.3 us  [from_behind(): return lax.ppermute(value, axis, pairs)]
    all_gather x1, waiting for transfers between devices: 8.14 us -> 0.01 us  [local(): group_rows = lax.all_gather(normed, 'tp', axis=0, tiled=True)]
    all_to_all x2 -> x1, starting transfers between devices: 11.1 us -> 3.64 us  [local(): lax.all_to_all(expert_rows(block), 'ep', split_axis=0, concat_axis=0, til...]
    ppermute x1 -> x4, waiting for transfers between devices: 0.98 us -> 6.87 us  [from_behind(): return lax.ppermute(value, axis, pairs)]
  transfers between devices with their start and end apart: 10 -> 11, of which waited for: 7 -> 6; matrix products, arithmetic and copies ran while one was open for 22% -> 31% of each run, Pallas kernels for 0% -> 0%
where the time goes in v2:
time: 233 us; the launch traced here: 232 us
  blocking collectives  80.4 us (35%)
  matrix products  57.2 us (25%)
  waiting for transfers between devices  35.4 us (15%)
  starting transfers between devices  22.3 us (10%)
  between operations  14.7 us (6%)
  other arithmetic  12.3 us (5%)
  local copies, waits for them, and re-layouts  9.4 us (4%)
    all_to_all x2, blocking collectives, local(): lax.all_to_all(block, 'ep', split_axis=0, concat_axis=0, tiled=True)  50.3 us
    all_to_all x1, blocking collectives, local(): lax.all_to_all(expert_rows(block), 'ep', split_axis=0, concat_axis=0, til...  30 us
    ppermute x4, starting transfers between devices, from_behind(): return lax.ppermute(value, axis, pairs)  18.3 us
    dot_general x2, matrix products, expert_rows(): jnp.einsum('osecf,efd->osecd', hidden, routed_down_weight, preferred_elem...  14.2 us
    reduce_scatter x1, waiting for transfers between devices, local(): lax.psum_scatter(jnp.concatenate([mix_term, moe_term], axis=1).reshape(tp...  13.4 us
    all_gather x2, waiting for transfers between devices, local(): gathered = [lax.all_gather(block, 'tp', axis=0) for block in arrived]  11.9 us
    dot_general x2, matrix products, expert_rows(): jnp.einsum('osecd,edf->osecf', sources, routed_gate_weight, preferred_ele...  8.17 us
    ppermute x4, waiting for transfers between devices, from_behind(): return lax.ppermute(value, axis, pairs)  6.87 us
  transfers between devices with their start and end apart: 11, of which 6 were waited for; matrix products, arithmetic and copies ran while one was open for 31% of the time, Pallas kernels for 0%

profile of v2, /device:TPU:0, one launch (start us, length us, event | category | flops | bytes accessed | tf_op | source)
XLA Modules:
  0.0 231.7 jit_solution(13960025605064493204)
XLA Ops:
  7.3 1.3 fusion.13
  8.6 2.0 fusion.15
  10.9 0.7 fusion.98
  11.8 1.4 convolution_convert_fusion.3
  13.3 27.3 %all_to_all.36 = bf16[8,24,2048]{2,1,0:T(8,128)(2,1)} all-to-all(bf16[8,24,2048]{2,1,0:T(8,128)(2,1)S(1)} %bitcast.295), channel_id=1, replica_groups=mesh['ep'=8,'tp'=4] {'ep'}, dimensions={0} | all-to-all | bytes 1572864 | tf_op jit(solution)/shard_map/all_to_all | solution.py:231
  40.7 3.3 %collective-permute-start = (bf16[3,1280]{1,0:T(4,128)(2,1)S(1)}, bf16[3,1280]{1,0:T(4,128)(2,1)S(1)}, u32[]{:S(2)}, u32[]{:S(2)}) collective-permute-start(bf16[3,1280]{1,0:T(4,128)(2,1)S(1)} %pad_maximum_fusion.4), channel_id=1, source_target_pairs={{0,4},{4,8},{8,12},{12,16},{16,20},{20,24},{24,28},{1,5},{5,9},{9,... | collective-permute-start | bytes 23048 | tf_op jit(solution)/shard_map/ppermute | solution.py:19
  44.5 1.0 collective-permute-done
  45.5 23.0 %all_to_all.37 = bf16[8,24,2048]{2,1,0:T(8,128)(2,1)} all-to-all(bf16[8,24,2048]{2,1,0:T(8,128)(2,1)S(1)} %bitcast.294), channel_id=1, replica_groups=mesh['ep'=8,'tp'=4] {'ep'}, dimensions={0} | all-to-all | bytes 1572864 | tf_op jit(solution)/shard_map/all_to_all | solution.py:231
  68.6 4.1 %convolution_bitcast_fusion.6 = f32[4,8,1,24,256]{4,3,1,0,2:T(8,128)} fusion(bf16[4,8,24,2048]{3,2,1,0:T(8,128)(2,1)} %bitcast.319, bf16[1,2048,256]{2,1,0:T(8,128)(2,1)} %param.38), kind=kOutput, calls=%fused_computation.20 | convolution fusion | flops 805306368 | bytes 4980736 | tf_op jit(solution)/shard_map/osecd,edf->osecf/dot_general | solution.py:257
  72.7 7.1 %convolution_convert_fusion = bf16[4,8,24,2048]{3,2,1,0:T(8,128)(2,1)} fusion(bf16[4,8,24,2048]{3,2,1,0:T(8,128)(2,1)} %bitcast.320, bf16[1,256,2048]{2,1,0:T(8,128)(2,1)S(1)} %copy-done, bf16[1,2048,256]{2,1,0:T(8,128)(2,1)S(1)} %copy-done.24, f32[4,8,1,24,256]{4,3,1,0,2:T(8,128)} %convolution_bitcast_fusion.6), kind=kOutput, calls=%fused_computation | convolution fusion | flops 1613365248 | bytes 9175040 | tf_op jit(solution)/shard_map/osecf,efd->osecd/dot_general | solution.py:264
  79.9 0.5 copy-done.27
  81.7 0.6 iota_compare_fusion.6
  82.4 0.6 bitcast_exponential_fusion
  84.4 2.1 fusion.24
  86.5 11.9 %all-gather.6.cloned.1.call-done = bf16[4,192,2048]{2,1,0:T(8,128)(2,1)} async-done(((bf16[1,192,2048]{2,1,0:T(8,128)(2,1)}), bf16[4,192,2048]{2,1,0:T(8,128)(2,1)}) %all-gather.6.cloned.1.call-update) | async-done | bytes 3145744 | tf_op jit(solution)/shard_map/all_gather | solution.py:232
  98.4 4.0 %convolution_bitcast_fusion.8 = f32[4,8,1,24,256]{4,3,1,0,2:T(8,128)} fusion(bf16[4,8,24,2048]{3,2,1,0:T(8,128)(2,1)} %bitcast.317, bf16[1,2048,256]{2,1,0:T(8,128)(2,1)} %param.38), kind=kOutput, calls=%fused_computation.22 | convolution fusion | flops 805306368 | bytes 4980736 | tf_op jit(solution)/shard_map/osecd,edf->osecf/dot_general | solution.py:257
  102.5 7.1 %convolution_convert_fusion.1 = bf16[4,8,24,2048]{3,2,1,0:T(8,128)(2,1)} fusion(bf16[4,8,24,2048]{3,2,1,0:T(8,128)(2,1)} %bitcast.318, bf16[1,256,2048]{2,1,0:T(8,128)(2,1)S(1)} %copy-done, bf16[1,2048,256]{2,1,0:T(8,128)(2,1)S(1)} %copy-done.25, f32[4,8,1,24,256]{4,3,1,0,2:T(8,128)} %convolution_bitcast_fusion.8), kind=kOutput, calls=%fused_computation.1 | convolution fusion | flops 1613365248 | bytes 9175040 | tf_op jit(solution)/shard_map/osecf,efd->osecd/dot_general | solution.py:264
  109.9 5.6 %fusion.32 = f32[16,1,64,128]{3,1,2,0:T(1,128)S(1)} fusion(f32[16,2,1,1]{1,2,3,0:T(1,128)S(1)} %copy.83, f32[2,16,64,128]{3,2,1,0:T(8,128)} %fusion.24), kind=kOutput, calls=%fused_computation.50 | convolution fusion | flops 3145728 | bytes 1572992 | tf_op jit(solution)/shard_map/gec,cgepn->gepn/dot_general | solution.py:136
  115.6 3.5 %collective-permute-start.1 = (bf16[1040,128]{1,0:T(8,128)(2,1)S(1)}, bf16[1040,128]{1,0:T(8,128)(2,1)S(1)}, u32[]{:S(2)}, u32[]{:S(2)}) collective-permute-start(bf16[1040,128]{1,0:T(8,128)(2,1)S(1)} %fusion.63), channel_id=1, source_target_pairs={{0,4},{4,8},{8,12},{12,16},{16,20},{20,24},{24,28},{1,5},{5,9},{9,... | collective-permute-start | bytes 798728 | tf_op jit(solution)/shard_map/ppermute | solution.py:19
  119.0 0.7 copy.75
  119.7 0.8 copy.89
  120.5 0.7 copy.73
  121.2 3.8 %collective-permute-done.1 = bf16[1040,128]{1,0:T(8,128)(2,1)S(1)} collective-permute-done((bf16[1040,128]{1,0:T(8,128)(2,1)S(1)}, bf16[1040,128]{1,0:T(8,128)(2,1)S(1)}, u32[]{:S(2)}, u32[]{:S(2)}) %collective-permute-start.1) | collective-permute-done | bytes 266272 | tf_op jit(solution)/shard_map/ppermute | solution.py:19
  125.3 0.8 add_convert_fusion.1
  126.2 5.3 %collective-permute-start.2 = (bf16[1040,128]{1,0:T(8,128)(2,1)S(1)}, bf16[1040,128]{1,0:T(8,128)(2,1)S(1)}, u32[]{:S(2)}, u32[]{:S(2)}) collective-permute-start(bf16[1040,128]{1,0:T(8,128)(2,1)S(1)} %fusion.64), channel_id=1, source_target_pairs={{0,8},{4,12},{8,16},{12,20},{16,24},{20,28},{1,9},{5,13},{9,17},{1... | collective-permute-start | bytes 798728 | tf_op jit(solution)/shard_map/ppermute | solution.py:19
  131.5 3.1 %fusion.120 = f32[512,128]{1,0:T(8,128)} fusion(bf16[512,2048]{1,0:T(8,128)(2,1)} %all-gather.4.cloned.1.call-done, bf16[2048,128]{1,0:T(8,128)(2,1)} %param.41), kind=kOutput, calls=%fused_computation.216 | convolution fusion | flops 268435456 | bytes 2883584 | tf_op jit(solution)/shard_map/dot_general | solution.py:235
  134.6 2.0 collective-permute-done.2
  136.8 0.6 pad_maximum_fusion.7
  137.4 0.8 copy.92
  138.2 0.7 add_exponential_fusion
  138.9 0.8 add_convert_fusion
  139.8 0.7 fusion.65
  140.6 6.2 %collective-permute-start.3 = (bf16[1040,128]{1,0:T(8,128)(2,1)}, bf16[1040,128]{1,0:T(8,128)(2,1)}, u32[]{:S(2)}, u32[]{:S(2)}) collective-permute-start(bf16[1040,128]{1,0:T(8,128)(2,1)} %fusion.65), channel_id=1, source_target_pairs={{0,16},{4,20},{8,24},{12,28},{1,17},{5,21},{9,25},{13,29},{2,18},{... | collective-permute-start | bytes 798728 | tf_op jit(solution)/shard_map/ppermute | solution.py:19
  146.7 5.7 %convolution_convert_fusion.2 = bf16[512,2048]{1,0:T(8,128)(2,1)} fusion(bf16[128,2048]{1,0:T(8,128)(2,1)} %param.43, f32[512,128]{1,0:T(8,128)} %fusion.120, bf16[512,2048]{1,0:T(8,128)(2,1)} %all-gather.4.cloned.1.call-done, bf16[2048,128]{1,0:T(8,128)(2,1)} %param.42), kind=kOutput, calls=%fused_computation.2 | convolution fusion | flops 538312704 | bytes 5505024 | tf_op jit(solution)/shard_map/dot_general | solution.py:238
  152.7 1.0 slice.163
  153.9 5.6 %fusion.10 = f32[2,16,64,128]{3,0,2,1:T(2,128)S(1)} fusion(f32[2,16,64,128]{3,2,1,0:T(8,128)} %fusion.24, f32[16,64,128]{2,1,0:T(8,128)S(1)} %fusion.52, f32[2,16]{0,1:T(8,128)S(1)} %copy-done.13, pred[2,2]{1,0:T(4,128)(4,1)S(1)} %copy-done.28, f32[16,2]{1,0:T(8,128)S(1)} %copy-done.14, f32[16,2]{1,0:T(8,128)S(1)} %bitcast.316), kind=kOutput, calls=%fused_computation.28 | convolution fusion | flops 6815872 | bytes 2621828 | tf_op jit(solution)/shard_map/gebc,cgepn->bgepn/dot_general | solution.py:134
  159.5 1.0 fusion.4
  160.5 2.0 fusion.3
  162.6 0.5 copy.80
  163.8 3.2 %convolution_convert_fusion.5 = bf16[128,2048]{1,0:T(8,128)(2,1)S(1)} fusion(bf16[1024,2048]{1,0:T(8,128)(2,1)} %param.33, f32[1024]{0:T(1024)S(1)} %copy-done.26, f32[128]{0:T(128)S(1)} %add_rsqrt_fusion, f32[128,1024]{1,0:T(8,128)S(1)} %reshape.463, bf16[128,1024]{1,0:T(8,128)(2,1)S(1)} %copy-done.8), kind=kOutput, calls=%fused_computation.11 | convolution fusion | flops 538312704 | bytes 5509632 | tf_op jit(solution)/shard_map/dot_general | solution.py:282
  167.0 1.7 pad_maximum_fusion
  168.8 30.0 %all_to_all.38 = bf16[8,24,2048]{2,1,0:T(8,128)(2,1)} all-to-all(bf16[8,24,2048]{2,1,0:T(8,128)(2,1)} %bitcast.301), channel_id=1, replica_groups=mesh['ep'=8,'tp'=4] {'ep'}, dimensions={0} | all-to-all | bytes 1572864 | tf_op jit(solution)/shard_map/all_to_all | solution.py:273
  198.8 3.6 %all-to-all-start.1 = ((bf16[8,24,2048]{2,1,0:T(8,128)(2,1)}), bf16[8,24,2048]{2,1,0:T(8,128)(2,1)S(1)}, u32[]{:S(2)}, u32[]{:S(2)}) async-start(bf16[8,24,2048]{2,1,0:T(8,128)(2,1)} %bitcast.302), calls=%async_computation.3 | async-start | bytes 1572864 | tf_op jit(solution)/shard_map/all_to_all | solution.py:273
  202.5 13.4 %reduce-scatter.4.cloned.1.call-done = bf16[160,2048]{1,0:T(8,128)(2,1)} async-done(((bf16[640,2048]{1,0:T(8,128)(2,1)}), bf16[160,2048]{1,0:T(8,128)(2,1)}) %reduce-scatter.4.cloned.1.call-update) | async-done | bytes 655376 | tf_op jit(solution)/shard_map/reduce_scatter | solution.py:286
  215.9 1.6 slice.164
  217.5 1.8 convolution_bitcast_fusion
  219.3 3.0 %all-to-all-done.1 = bf16[8,24,2048]{2,1,0:T(8,128)(2,1)S(1)} async-done(((bf16[8,24,2048]{2,1,0:T(8,128)(2,1)}), bf16[8,24,2048]{2,1,0:T(8,128)(2,1)S(1)}, u32[]{:S(2)}, u32[]{:S(2)}) %all-to-all-start.1) | async-done | bytes 786464 | tf_op jit(solution)/shard_map/all_to_all | solution.py:273
  222.3 2.5 %fusion.2 = bf16[128,2048]{1,0:T(8,128)(2,1)} fusion(f32[128,2048]{1,0:T(8,128)S(1)} %convolution_bitcast_fusion, bf16[8,24,2048]{2,1,0:T(8,128)(2,1)S(1)} %all-to-all-done.1, bf16[160,2048]{1,0:T(8,128)(2,1)} %reduce-scatter.4.cloned.1.call-done, f32[8,128]{1,0:T(8,128)S(1)} %select_reduce_fusion, s32[8,128]{1,0:T(8,128)S(1)} %convolution_convert_fusion.6, ...), kind=kOutput, calls=%fused_computation.10 | convolution fusion | flops 605102080 | bytes 2892800 | tf_op jit(solution)/shard_map/sr,sd->rd/dot_general | solution.py:277
  (140 shorter events, 5.9 us)
Async XLA Ops:
  7.2 65.5 %copy-start = (bf16[1,256,2048]{2,1,0:T(8,128)(2,1)S(1)}, bf16[1,256,2048]{2,1,0:T(8,128)(2,1)}, u32[]{:S(2)}) copy-start(bf16[1,256,2048]{2,1,0:T(8,128)(2,1)} %param.40) | copy-start | bytes 3145732
  7.2 33.5 %copy-start.7 = (bf16[128,1024]{1,0:T(8,128)(2,1)S(1)}, bf16[128,1024]{1,0:T(8,128)(2,1)}, u32[]{:S(2)}) copy-start(bf16[128,1024]{1,0:T(8,128)(2,1)} %param.22) | copy-start | bytes 786436
  7.2 33.5 %copy-start.9 = (bf16[128,128]{1,0:T(8,128)(2,1)S(1)}, bf16[128,128]{1,0:T(8,128)(2,1)}, u32[]{:S(2)}) copy-start(bf16[128,128]{1,0:T(8,128)(2,1)} %param.23) | copy-start | bytes 98308
  7.2 33.5 %copy-start.10 = (bf16[128,128]{1,0:T(8,128)(2,1)S(1)}, bf16[128,128]{1,0:T(8,128)(2,1)}, u32[]{:S(2)}) copy-start(bf16[128,128]{1,0:T(8,128)(2,1)} %param.24) | copy-start | bytes 98308
  7.2 38.2 %all-gather.4.cloned.1.call-start = ((), (), s32[]{:S(2)}) async-start(), calls=%async_computation.7 | async-start | bytes 2621440 | tf_op jit(solution)/shard_map/all_gather | solution.py:226
  10.6 33.5 %copy-start.2 = (bf16[128,2048]{1,0:T(8,128)(2,1)S(1)}, bf16[128,2048]{1,0:T(8,128)(2,1)}, u32[]{:S(2)}) copy-start(bf16[128,2048]{1,0:T(8,128)(2,1)} %fusion.15) | copy-start | bytes 1572868
  10.6 57.9 %all-gather.8.cloned.1.call-start = ((), (), s32[]{:S(2)}) async-start(), calls=%async_computation.11 | async-start | bytes 3932160 | tf_op jit(solution)/shard_map/all_gather | solution.py:232
  10.7 0.9 copy-start.21
  40.6 57.8 %all-gather.6.cloned.1.call-start = ((), (), s32[]{:S(2)}) async-start(), calls=%async_computation.9 | async-start | bytes 3932160 | tf_op jit(solution)/shard_map/all_gather | solution.py:232
  40.7 4.7 %collective-permute-start = (bf16[3,1280]{1,0:T(4,128)(2,1)S(1)}, bf16[3,1280]{1,0:T(4,128)(2,1)S(1)}, u32[]{:S(2)}, u32[]{:S(2)}) collective-permute-start(bf16[3,1280]{1,0:T(4,128)(2,1)S(1)} %pad_maximum_fusion.4), channel_id=1, source_target_pairs={{0,4},{4,8},{8,12},{12,16},{16,20},{20,24},{24,28},{1,5},{5,9},{9,... | collective-permute-start | bytes 23048 | tf_op jit(solution)/shard_map/ppermute | solution.py:19
  68.5 4.2 %copy-start.24 = (bf16[1,2048,256]{2,1,0:T(8,128)(2,1)S(1)}, bf16[1,2048,256]{2,1,0:T(8,128)(2,1)}, u32[]{:S(2)}) copy-start(bf16[1,2048,256]{2,1,0:T(8,128)(2,1)} %param.39) | copy-start | bytes 3145732
  68.5 100.3 %reduce-scatter.8.cloned.1.call-start = ((), (), s32[]{:S(2)}) async-start(), calls=%async_computation.12 | async-start | bytes 3932160 | tf_op jit(solution)/shard_map/reduce_scatter | solution.py:267
  79.8 0.7 copy-start.27
  79.8 0.7 copy-start.15
  79.8 0.7 copy-start.16
  79.8 3.2 %copy-start.18 = (bf16[4,128]{1,0:T(4,128)(2,1)S(1)}, bf16[4,128]{1,0:T(4,128)(2,1)}, u32[]{:S(2)}) copy-start(bf16[4,128]{1,0:T(4,128)(2,1)} %param.30) | copy-start | bytes 3076
  79.8 3.2 %copy-start.19 = (bf16[4,128]{1,0:T(4,128)(2,1)S(1)}, bf16[4,128]{1,0:T(4,128)(2,1)}, u32[]{:S(2)}) copy-start(bf16[4,128]{1,0:T(4,128)(2,1)} %param.31) | copy-start | bytes 3076
  79.8 3.2 %copy-start.11 = (bf16[4,1024]{1,0:T(4,128)(2,1)S(1)}, bf16[4,1024]{1,0:T(4,128)(2,1)}, u32[]{:S(2)}) copy-start(bf16[4,1024]{1,0:T(4,128)(2,1)} %param.29) | copy-start | bytes 24580
  79.8 119.0 %reduce-scatter.6.cloned.1.call-start = ((), (), s32[]{:S(2)}) async-start(), calls=%async_computation.10 | async-start | bytes 3932160 | tf_op jit(solution)/shard_map/reduce_scatter | solution.py:267
  84.4 18.1 %copy-start.5 = (f32[128,128]{1,0:T(8,128)}, f32[128,128]{1,0:T(8,128)S(1)}, u32[]{:S(2)}) copy-start(f32[128,128]{1,0:T(8,128)S(1)} %get-tuple-element.38) | copy-start | bytes 196612
  86.5 16.0 %copy-start.25 = (bf16[1,2048,256]{2,1,0:T(8,128)(2,1)S(1)}, bf16[1,2048,256]{2,1,0:T(8,128)(2,1)}, u32[]{:S(2)}) copy-start(bf16[1,2048,256]{2,1,0:T(8,128)(2,1)} %param.39) | copy-start | bytes 3145732
  109.6 106.3 %reduce-scatter.4.cloned.1.call-start = ((), (), s32[]{:S(2)}) async-start(), calls=%async_computation.8 | async-start | bytes 3276800 | tf_op jit(solution)/shard_map/reduce_scatter | solution.py:286
  115.6 9.5 %collective-permute-start.1 = (bf16[1040,128]{1,0:T(8,128)(2,1)S(1)}, bf16[1040,128]{1,0:T(8,128)(2,1)S(1)}, u32[]{:S(2)}, u32[]{:S(2)}) collective-permute-start(bf16[1040,128]{1,0:T(8,128)(2,1)S(1)} %fusion.63), channel_id=1, source_target_pairs={{0,4},{4,8},{8,12},{12,16},{16,20},{20,24},{24,28},{1,5},{5,9},{9,... | collective-permute-start | bytes 798728 | tf_op jit(solution)/shard_map/ppermute | solution.py:19
  126.2 10.5 %collective-permute-start.2 = (bf16[1040,128]{1,0:T(8,128)(2,1)S(1)}, bf16[1040,128]{1,0:T(8,128)(2,1)S(1)}, u32[]{:S(2)}, u32[]{:S(2)}) collective-permute-start(bf16[1040,128]{1,0:T(8,128)(2,1)S(1)} %fusion.64), channel_id=1, source_target_pairs={{0,8},{4,12},{8,16},{12,20},{16,24},{20,28},{1,9},{5,13},{9,17},{1... | collective-permute-start | bytes 798728 | tf_op jit(solution)/shard_map/ppermute | solution.py:19
  136.8 1.4 copy-start.17
  138.2 1.6 copy-start.3
  139.8 12.7 %copy-start.6 = (f32[128,128]{1,0:T(8,128)S(1)}, f32[128,128]{1,0:T(8,128)}, u32[]{:S(2)}) copy-start(f32[128,128]{1,0:T(8,128)} %copy-done.5) | copy-start | bytes 196612
  140.5 13.1 %copy-start.4 = (f32[1024,128]{1,0:T(8,128)S(1)}, f32[1024,128]{1,0:T(8,128)}, u32[]{:S(2)}) copy-start(f32[1024,128]{1,0:T(8,128)} %copy-done.3) | copy-start | bytes 1572868
  140.5 13.3 %copy-start.12 = (f32[1,16,2,1]{2,1,3,0:T(8,128)S(1)}, f32[1,16,2,1]{2,1,3,0:T(8,128)}, u32[]{:S(2)}) copy-start(f32[1,16,2,1]{2,1,3,0:T(8,128)} %copy.89) | copy-start | bytes 388
  140.5 13.3 %copy-start.13 = (f32[2,16]{0,1:T(8,128)S(1)}, f32[2,16]{0,1:T(8,128)}, u32[]{:S(2)}) copy-start(f32[2,16]{0,1:T(8,128)} %copy.75) | copy-start | bytes 388
  140.5 13.3 %copy-start.14 = (f32[16,2]{1,0:T(8,128)S(1)}, f32[16,2]{1,0:T(8,128)}, u32[]{:S(2)}) copy-start(f32[16,2]{1,0:T(8,128)} %copy.73) | copy-start | bytes 388
  140.6 13.3 %copy-start.28 = (pred[2,2]{1,0:T(4,128)(4,1)S(1)}, pred[2,2]{1,0:T(4,128)(4,1)}, u32[]{:S(2)}) copy-start(pred[2,2]{1,0:T(4,128)(4,1)} %iota_compare_fusion.6) | copy-start | bytes 16
  140.6 12.1 %collective-permute-start.3 = (bf16[1040,128]{1,0:T(8,128)(2,1)}, bf16[1040,128]{1,0:T(8,128)(2,1)}, u32[]{:S(2)}, u32[]{:S(2)}) collective-permute-start(bf16[1040,128]{1,0:T(8,128)(2,1)} %fusion.65), channel_id=1, source_target_pairs={{0,16},{4,20},{8,24},{12,28},{1,17},{5,21},{9,25},{13,29},{2,18},{... | collective-permute-start | bytes 798728 | tf_op jit(solution)/shard_map/ppermute | solution.py:19
  160.5 3.3 %copy-start.26 = (f32[1024]{0:T(1024)S(1)}, f32[1024]{0:T(1024)}, u32[]{:S(2)}) copy-start(f32[1024]{0:T(1024)} %param.32) | copy-start | bytes 12292
  162.6 1.0 copy-start.8
  163.8 3.2 %copy-start.1 = (bf16[512,2048]{1,0:T(8,128)(2,1)S(1)}, bf16[512,2048]{1,0:T(8,128)(2,1)}, u32[]{:S(2)}) copy-start(bf16[512,2048]{1,0:T(8,128)(2,1)} %convolution_convert_fusion.2) | copy-start | bytes 6291460
  168.7 33.7 %copy-start.23 = (bf16[128,2]{0,1:T(2,128)(2,1)S(1)}, bf16[128,2]{0,1:T(2,128)(2,1)}, u32[]{:S(2)}) copy-start(bf16[128,2]{0,1:T(2,128)(2,1)} %param.37) | copy-start | bytes 1540
  168.7 33.8 %copy-start.20 = (s32[128,2]{0,1:T(2,128)S(1)}, s32[128,2]{0,1:T(2,128)}, u32[]{:S(2)}) copy-start(s32[128,2]{0,1:T(2,128)} %param.36) | copy-start | bytes 3076
  168.7 48.8 %copy-start.22 = (s32[24]{0:T(128)S(1)}, s32[24]{0:T(128)}, u32[]{:S(2)}) copy-start(s32[24]{0:T(128)} %copy-done.21) | copy-start | bytes 292
  198.8 23.5 %all-to-all-start.1 = ((bf16[8,24,2048]{2,1,0:T(8,128)(2,1)}), bf16[8,24,2048]{2,1,0:T(8,128)(2,1)S(1)}, u32[]{:S(2)}, u32[]{:S(2)}) async-start(bf16[8,24,2048]{2,1,0:T(8,128)(2,1)} %bitcast.302), calls=%async_computation.3 | async-start | bytes 1572864 | tf_op jit(solution)/shard_map/all_to_all | solution.py:273
Sparse Core Ops, SparseCore 0:
  10.8 25.2 all-gather.3
  40.7 27.5 all-gather.7
  69.9 28.4 all-gather.5
  100.8 37.9 reduce-scatter.7
  141.2 37.8 reduce-scatter.5
  181.4 34.4 reduce-scatter.3
